TPU v7x, 256 devices: a whole 4x4x8 slice. The times are simulated.
256 devices in a mesh: ep: 64 (over z, y, core), tp: 4 (over x).
Axes of the slice: x: 4, y: 4, z: 8, core: 2. Of those that a mesh axis runs over, the one named last changes fastest.
Arguments:
- query: bfloat16 [8192, 1536], P('ep', 'tp'), may hold values from -136 to 136
- latent: bfloat16 [8192, 512], P(('ep', 'tp')), may hold values from -6 to 6
- rope_key: bfloat16 [8192, 32], P(('ep', 'tp')), may hold values from -6 to 6
- latent_gain: float32 [512], replicated, may hold values from 0.1 to 1.9
- key_up: bfloat16 [512, 1024], P(None, 'tp'), may hold values from -0.25 to 0.25
- value_up: bfloat16 [512, 1024], P(None, 'tp'), may hold values from -2 to 2
- out_proj: bfloat16 [1024, 2048], replicated, may hold values from -0.1875 to 0.1875
- tokens: bfloat16 [16384, 2048], P(('ep', 'tp')), may hold values from -6 to 6
- moe_gain: float32 [2048], replicated, may hold values from 0.1 to 1.9
- routes: int32 [16384, 2], P(('ep', 'tp')), may hold values from 0 to 63, all different within a row; in each aligned block of 64 rows (0 to 63, 64 to 127, ...) at most 4 rows name the same one
- group_prob: float32 [16384], P(('ep', 'tp')), may hold values from 0.25 to 1
- expert_prob: float32 [16384, 2], P(('ep', 'tp')), may hold values from 0.02 to 1
- w_gate: bfloat16 [64, 2048, 1024], P('ep', None, 'tp'), may hold values from -0.125 to 0.125
- w_up: bfloat16 [64, 2048, 1024], P('ep', None, 'tp'), may hold values from -0.125 to 0.125
- w_down: bfloat16 [64, 1024, 2048], P('ep', 'tp'), may hold values from -0.1875 to 0.1875
Outputs:
- mixed: bfloat16 [8192, 2048], P(('ep', 'tp'))
- moe_out: bfloat16 [16384, 2048], P(('ep', 'tp'))
Inputs may be any that keep to these rules, and one draw needn't show every extreme that they name: `routes`: each row names 2 different experts; within the rows of one device no expert is named more than 4 times.
All inputs are finite; a program needn't handle non-finite values.
Results may differ from a plain program's by a relative error of at most 0.025.
Values may be sent and summed in bfloat16 or wider, within the bound.
A program may use at most 128 MiB of HBM per device.

v0:
```python
import math

import jax
import jax.numpy as jnp
from jax import lax
from jax.sharding import PartitionSpec as P

NOPE = 64
ROPE_DIM = 32
V_DIM = 64


epsilon = 1e-06
rope_base = 10000.0
masked_value = -1e30


def in_one_piece(arrays, axis, dim, along):
    both = jnp.concatenate(arrays, axis=along)
    out, at, done = (lax.all_gather(both, axis, axis=dim, tiled=True), 0, [])
    for a in arrays:
        done.append(lax.slice_in_dim(out, at, at + a.shape[along], axis=along))
        at += a.shape[along]
    return tuple(done)


def split_up(value, dim, devices):
    before, after = (value.shape[:dim], value.shape[dim + 1 :])
    return jnp.moveaxis(value.reshape(*before, devices, -1, *after), dim, 0)


def sent_and_summed(value, axis, dim):
    devices = lax.axis_size(axis)
    parts = lax.all_to_all(split_up(value, dim, devices), axis, 0, 0, tiled=True)
    return jnp.sum(parts.astype(jnp.float32), axis=0)


def rms_scale(values, gain):
    widened = values.astype(jnp.float32)
    return widened * lax.rsqrt(jnp.mean(widened * widened, axis=-1, keepdims=True) + epsilon) * gain


def tables(positions, rope_width):
    half_width = rope_width // 2
    inverse = rope_base ** (-2.0 * jnp.arange(half_width, dtype=jnp.float32) / rope_width)
    angles = positions.astype(jnp.float32)[:, None] * inverse[None, :]
    return (jnp.cos(angles), jnp.sin(angles))


def rotate(values, cosine, sine):
    half_width = values.shape[-1] // 2
    lower = values[..., :half_width]
    upper = values[..., half_width:]
    return jnp.concatenate([lower * cosine - upper * sine, lower * sine + upper * cosine], axis=-1)


def keep_state(state_in):
    return state_in


def attend_block(running, query_rot, query_pos, key_part, value_part, rope_part):
    amount = key_part.shape[0]
    span_rows = math.gcd(amount, 1024)
    head_count = query_rot.shape[1]
    scale_factor = query_rot.shape[2] ** (-0.5)
    last_query = query_pos[-1]

    def update(state, block_at):
        row_begin = block_at * span_rows
        keys_here = lax.dynamic_slice_in_dim(key_part, row_begin, span_rows, 0).reshape(
            span_rows, head_count, -1
        )
        values_here = lax.dynamic_slice_in_dim(value_part, row_begin, span_rows, 0).reshape(
            span_rows, head_count, -1
        )
        rope_here = lax.dynamic_slice_in_dim(rope_part, row_begin, span_rows, 0)
        key_pos = row_begin + jnp.arange(span_rows, dtype=jnp.int32)

        def advance(state_in):
            top_old, totals, weighted = state_in
            shared = jnp.broadcast_to(
                rope_here[:, None, :], (span_rows, head_count, rope_here.shape[1])
            )
            full_keys = jnp.concatenate([keys_here, shared], axis=-1)
            scores = (
                jnp.einsum("qhd,khd->hqk", query_rot, full_keys, preferred_element_type=jnp.float32)
                * scale_factor
            )
            allowed = key_pos[None, :] <= query_pos[:, None]
            scores = jnp.where(allowed[None], scores, masked_value)
            top_new = jnp.maximum(top_old, jnp.max(scores, axis=-1))
            raised = jnp.where(allowed[None], jnp.exp(scores - top_new[..., None]), 0.0)
            factor = jnp.exp(top_old - top_new)
            totals = totals * factor + jnp.sum(raised, axis=-1)
            weighted = weighted * factor[..., None] + jnp.einsum(
                "hqk,khd->hqd",
                raised.astype(jnp.bfloat16),
                values_here,
                preferred_element_type=jnp.float32,
            )
            return (top_new, totals, weighted)

        return (lax.cond(key_pos[0] <= last_query, advance, keep_state, state), None)

    running, _ = lax.scan(update, running, jnp.arange(amount // span_rows))
    return running


def mixer_half(query, latent, rope_key, latent_gain, key_up, value_up, out_proj):
    query_rows = query.shape[0]
    own_rows = latent.shape[0]
    query_start = lax.axis_index("ep") * query_rows
    key_start = query_start + lax.axis_index("tp") * own_rows
    head_count = query.shape[1] // (NOPE + ROPE_DIM)
    normed = rms_scale(latent, latent_gain).astype(jnp.bfloat16)
    key_cos, key_sin = tables(key_start + jnp.arange(own_rows, dtype=jnp.int32), ROPE_DIM)
    rotated_key = rotate(rope_key.astype(jnp.float32), key_cos, key_sin).astype(jnp.bfloat16)
    query_pos = query_start + jnp.arange(query_rows, dtype=jnp.int32)
    query_cos, query_sin = tables(query_pos, ROPE_DIM)
    query_heads = query.reshape(query_rows, head_count, NOPE + ROPE_DIM)
    turned = rotate(
        query_heads[..., NOPE:].astype(jnp.float32), query_cos[:, None, :], query_sin[:, None, :]
    ).astype(jnp.bfloat16)
    query_rot = jnp.concatenate([query_heads[..., :NOPE], turned], axis=-1)
    last_query = query_start + query_rows - 1
    initial = (
        jnp.full((head_count, query_rows), masked_value, jnp.float32),
        jnp.zeros((head_count, query_rows), jnp.float32),
        jnp.zeros((head_count, query_rows, V_DIM), jnp.float32),
    )
    group_latent, group_rope = in_one_piece((normed, rotated_key), "tp", 0, 1)
    key_part = jnp.dot(group_latent, key_up, preferred_element_type=jnp.float32).astype(
        jnp.bfloat16
    )
    value_part = jnp.dot(group_latent, value_up, preferred_element_type=jnp.float32).astype(
        jnp.bfloat16
    )
    shard_rows = in_one_piece((key_part, value_part, group_rope), "ep", 0, 1)

    def compute(state_in):
        return attend_block(
            state_in, query_rot, query_pos, shard_rows[0], shard_rows[1], shard_rows[2]
        )

    running = lax.cond(jnp.int32(0) <= last_query, compute, keep_state, initial)
    totals = running[1]
    weighted = running[2]
    attention = (
        (weighted / totals[..., None])
        .transpose(1, 0, 2)
        .reshape(query_rows, head_count * V_DIM)
        .astype(jnp.bfloat16)
    )
    own_attention = lax.all_to_all(attention, "tp", split_axis=0, concat_axis=1, tiled=True)
    return jnp.dot(own_attention, out_proj, preferred_element_type=jnp.float32).astype(jnp.bfloat16)


def expert_half(tokens, moe_gain, routes, group_prob, expert_prob, w_gate, w_up, w_down):
    row_count, model_width = tokens.shape
    top_count = routes.shape[1]
    expert_count = lax.axis_size("ep")
    capacity = 2 * top_count * row_count // expert_count
    normed = rms_scale(tokens, moe_gain).astype(jnp.bfloat16)
    flat_routes = routes.reshape(-1)
    onehot = (flat_routes[:, None] == jnp.arange(expert_count, dtype=jnp.int32)[None, :]).astype(
        jnp.int32
    )
    earlier = jnp.cumsum(onehot, axis=0) - onehot
    slot_index = jnp.sum(earlier * onehot, axis=1)
    target = flat_routes * capacity + slot_index
    owner = target[None, :] == jnp.arange(expert_count * capacity, dtype=jnp.int32)[:, None]
    dispatch_table = jnp.any(
        owner.reshape(expert_count * capacity, row_count, top_count), axis=2
    ).astype(jnp.bfloat16)
    outgoing = jnp.dot(dispatch_table, normed, preferred_element_type=jnp.float32).astype(
        jnp.bfloat16
    )
    outgoing = outgoing.reshape(expert_count, capacity, model_width)
    arrived = lax.all_to_all(outgoing, "ep", split_axis=0, concat_axis=0, tiled=True)
    sources, slots, _ = arrived.shape
    flat_rows = arrived.reshape(sources * slots, model_width)
    shard_rows = lax.all_gather(flat_rows, "tp", axis=0, tiled=True)
    gate_values = jnp.dot(shard_rows, w_gate[0], preferred_element_type=jnp.float32)
    up_values = jnp.dot(shard_rows, w_up[0], preferred_element_type=jnp.float32)
    hidden = (jax.nn.silu(gate_values) * up_values).astype(jnp.bfloat16)

    def lower(offset, amount):
        return jnp.dot(hidden, w_down[0], preferred_element_type=jnp.float32)

    summed = sent_and_summed(
        lower(jnp.int32(0), sources * slots * lax.axis_size("tp")).astype(jnp.bfloat16), "tp", 0
    )
    result = summed.astype(jnp.bfloat16).reshape(sources, slots, model_width)
    returned = lax.all_to_all(result, "ep", split_axis=0, concat_axis=0, tiled=True)
    returned_flat = returned.reshape(expert_count * capacity, model_width)
    picked = returned_flat[target].reshape(row_count, top_count, model_width).astype(jnp.float32)
    shares = group_prob[:, None] * expert_prob / jnp.sum(expert_prob, axis=1, keepdims=True)
    return jnp.sum(shares[:, :, None] * picked, axis=1).astype(jnp.bfloat16)


def body(
    query,
    latent,
    rope_key,
    latent_gain,
    key_up,
    value_up,
    out_proj,
    tokens,
    moe_gain,
    routes,
    group_prob,
    expert_prob,
    w_gate,
    w_up,
    w_down,
):
    mixed = mixer_half(query, latent, rope_key, latent_gain, key_up, value_up, out_proj)
    moe_out = expert_half(tokens, moe_gain, routes, group_prob, expert_prob, w_gate, w_up, w_down)
    return (mixed, moe_out)


def solution(mesh):
    return jax.shard_map(
        body,
        mesh=mesh,
        in_specs=(
            P("ep", "tp"),
            P(("ep", "tp"), None),
            P(("ep", "tp"), None),
            P(),
            P(None, "tp"),
            P(None, "tp"),
            P(),
            P(("ep", "tp"), None),
            P(),
            P(("ep", "tp"), None),
            P(("ep", "tp")),
            P(("ep", "tp"), None),
            P("ep", None, "tp"),
            P("ep", None, "tp"),
            P("ep", "tp", None),
        ),
        out_specs=(P(("ep", "tp"), None), P(("ep", "tp"), None)),
        check_vma=False,
    )
```

profile of v0, /device:TPU:224, one launch (start us, length us, event | category | flops | bytes accessed | tf_op | source)
XLA Modules:
  0.0 333.0 jit_solution(12804921602035847933)
XLA Ops:
  12.0 36.0 %all_to_all.31 = bf16[64,4,2048]{2,1,0:T(4,128)(2,1)S(1)} all-to-all(bf16[64,4,2048]{2,1,0:T(4,128)(2,1)S(1)} %reshape.209), channel_id=1, replica_groups=mesh['ep'=64,'tp'=4] {'ep'}, dimensions={0} | all-to-all | bytes 2097152 | tf_op jit(solution)/shard_map/all_to_all | solution.py:179
  50.0 12.4 %all_gather.9 = bf16[128,544]{1,0:T(8,128)(2,1)S(1)} all-gather(bf16[32,544]{1,0:T(8,128)(2,1)S(1)} %pad_maximum_fusion.2), channel_id=1, replica_groups=mesh['ep'=64,'tp'=4] {'tp'}, dimensions={0}, use_global_device_ids=true | all-gather | bytes 174080 | tf_op jit(solution)/shard_map/all_gather | solution.py:20
  63.6 35.2 %all-gather.5.cloned.1.call-done = bf16[1024,2048]{1,0:T(8,128)(2,1)} async-done(((bf16[256,2048]{1,0:T(8,128)(2,1)}), bf16[1024,2048]{1,0:T(8,128)(2,1)}) %all-gather.5.cloned.1.call-update) | async-done | bytes 4194320 | tf_op jit(solution)/shard_map/all_gather | solution.py:182
  98.8 4.4 %fusion.20 = f32[1024,256]{1,0:T(8,128)} fusion(bf16[1024,2048]{1,0:T(8,128)(2,1)} %all-gather.5.cloned.1.call-done, bf16[1,2048,256]{2,1,0:T(8,128)(2,1)S(1)} %copy-done.9), kind=kOutput, calls=%fused_computation.36 | convolution fusion | flops 1073741824 | bytes 6291456 | tf_op jit(solution)/shard_map/dot_general | solution.py:183
  103.2 8.8 %convolution_convert_fusion = bf16[1024,2048]{1,0:T(8,128)(2,1)} fusion(bf16[1024,2048]{1,0:T(8,128)(2,1)} %all-gather.5.cloned.1.call-done, bf16[1,256,2048]{2,1,0:T(8,128)(2,1)S(1)} %copy-done, bf16[1,2048,256]{2,1,0:T(8,128)(2,1)S(1)} %copy-done.10, f32[1024,256]{1,0:T(8,128)} %fusion.20), kind=kOutput, calls=%fused_computation.27 | convolution fusion | flops 2151153664 | bytes 11534336 | tf_op jit(solution)/shard_map/dot_general | solution.py:188
  112.0 54.6 %all_to_all.32 = bf16[4,256,2048]{2,1,0:T(8,128)(2,1)} all-to-all(bf16[4,256,2048]{2,1,0:T(8,128)(2,1)} %bitcast.54), channel_id=1, replica_groups=mesh['ep'=64,'tp'=4] {'tp'}, dimensions={0} | all-to-all | bytes 8388608 | tf_op jit(solution)/shard_map/all_to_all | solution.py:34
  166.6 3.4 %reduce_sum.78 = bf16[256,2048]{1,0:T(8,128)(2,1)S(1)} reduce(bf16[4,256,2048]{2,1,0:T(8,128)(2,1)} %all_to_all.32, bf16[]{:T(256)} %constant.106.clone.1), dimensions={0}, to_apply=%region_14.15 | reduce | flops 1572864 | bytes 5242882 | tf_op jit(solution)/shard_map/reduce_sum | solution.py:35
  171.3 10.0 %all-to-all-start.3 = ((bf16[64,4,2048]{2,1,0:T(4,128)(2,1)}), bf16[64,4,2048]{2,1,0:T(4,128)(2,1)S(1)}, u32[]{:S(2)}, u32[]{:S(2)}) async-start(bf16[64,4,2048]{2,1,0:T(4,128)(2,1)} %reshape.212), calls=%async_computation.3 | async-start | bytes 2097152 | tf_op jit(solution)/shard_map/all_to_all | solution.py:194
  181.9 26.5 %all-to-all-done.3 = bf16[64,4,2048]{2,1,0:T(4,128)(2,1)S(1)} async-done(((bf16[64,4,2048]{2,1,0:T(4,128)(2,1)}), bf16[64,4,2048]{2,1,0:T(4,128)(2,1)S(1)}, u32[]{:S(2)}, u32[]{:S(2)}) %all-to-all-start.3) | async-done | bytes 1048608 | tf_op jit(solution)/shard_map/all_to_all | solution.py:194
  210.4 101.0 %conditional.2 = (f32[4,128]{1,0:T(4,128)}, f32[4,128,64]{1,2,0:T(8,128)}) conditional(s32[]{:T(128)} %convert_element_type.89, () %tuple.36, (bf16[8192,544]{1,0:T(8,128)(2,1)}, s32[]{:T(128)}, s32[128]{0:T(128)S(1)}, bf16[128,4,96]{0,2,1:T(8,128)(2,1)S(1)}) %tuple.37), branch_computations={%region_1.0_spmd, %region_2.9_spmd} | conditional | flops 176359552 | bytes 46872600 | solution.py:145
  210.4 12.9 %copy.45 = bf16[8192,544]{0,1:T(8,128)(2,1)} copy(bf16[8192,544]{1,0:T(8,128)(2,1)} %get-tuple-element.221) | data formatting | bytes 17825792 | tf_op jit(solution)/shard_map
  223.3 6.1 %fusion.53 = (bf16[8192,256]{0,1:T(8,128)(2,1)}, bf16[8192,256]{0,1:T(8,128)(2,1)}) fusion(bf16[8192,544]{0,1:T(8,128)(2,1)} %copy.45), kind=kLoop, calls=%fused_computation.97 | loop fusion | bytes 16777216 | tf_op jit(solution)/shard_map/slice | solution.py:22
  232.3 79.0 %while.13 = (s32[]{:T(128)}, f32[4,128]{1,0:T(4,128)S(1)}, f32[4,128]{1,0:T(4,128)}, f32[4,128,64]{1,2,0:T(8,128)}, s32[8]{0:T(128)S(1)}, /*index=5*/s32[]{:T(12...) while((s32[]{:T(128)}, f32[4,128]{1,0:T(4,128)S(1)}, ...), condition=%wide.region_8.8_spmd, body=%wide.region_3.7_spmd.sunk | while | flops 176359424 | bytes 11084641 | solution.py:105
  235.2 7.0 %conditional.4 = ((f32[4,128]{1,0:T(4,128)S(1)}, f32[4,128]{1,0:T(4,128)}, f32[4,128,64]{1,2,0:T(8,128)})) conditional(s32[]{:T(128)} %convert_element_type.152, (f32[4,128]{1,0:T(4,128)S(1)}, f32[4,128]{1,0:T(4,128)}, f32[4,128,64]{1,2,0:T(8,128)}) %tuple.61, (s32[1024]{0:T(1024)S(1)}, s32[128]{0:T(128)S(1)}, s32[]{:T(128)}, ...), branch_computations={%region_4.3_spmd, %region_5.6_spmd} | conditional | flops 176358400 | bytes 11080266 | solution.py:103
  245.1 7.0 %conditional.4 = ((f32[4,128]{1,0:T(4,128)S(1)}, f32[4,128]{1,0:T(4,128)}, f32[4,128,64]{1,2,0:T(8,128)})) conditional(s32[]{:T(128)} %convert_element_type.152, (f32[4,128]{1,0:T(4,128)S(1)}, f32[4,128]{1,0:T(4,128)}, f32[4,128,64]{1,2,0:T(8,128)}) %tuple.61, (s32[1024]{0:T(1024)S(1)}, s32[128]{0:T(128)S(1)}, s32[]{:T(128)}, ...), branch_computations={%region_4.3_spmd, %region_5.6_spmd} | conditional | flops 176358400 | bytes 11080266 | solution.py:103
  255.0 7.0 %conditional.4 = ((f32[4,128]{1,0:T(4,128)S(1)}, f32[4,128]{1,0:T(4,128)}, f32[4,128,64]{1,2,0:T(8,128)})) conditional(s32[]{:T(128)} %convert_element_type.152, (f32[4,128]{1,0:T(4,128)S(1)}, f32[4,128]{1,0:T(4,128)}, f32[4,128,64]{1,2,0:T(8,128)}) %tuple.61, (s32[1024]{0:T(1024)S(1)}, s32[128]{0:T(128)S(1)}, s32[]{:T(128)}, ...), branch_computations={%region_4.3_spmd, %region_5.6_spmd} | conditional | flops 176358400 | bytes 11080266 | solution.py:103
  264.9 7.0 %conditional.4 = ((f32[4,128]{1,0:T(4,128)S(1)}, f32[4,128]{1,0:T(4,128)}, f32[4,128,64]{1,2,0:T(8,128)})) conditional(s32[]{:T(128)} %convert_element_type.152, (f32[4,128]{1,0:T(4,128)S(1)}, f32[4,128]{1,0:T(4,128)}, f32[4,128,64]{1,2,0:T(8,128)}) %tuple.61, (s32[1024]{0:T(1024)S(1)}, s32[128]{0:T(128)S(1)}, s32[]{:T(128)}, ...), branch_computations={%region_4.3_spmd, %region_5.6_spmd} | conditional | flops 176358400 | bytes 11080266 | solution.py:103
  274.8 7.0 %conditional.4 = ((f32[4,128]{1,0:T(4,128)S(1)}, f32[4,128]{1,0:T(4,128)}, f32[4,128,64]{1,2,0:T(8,128)})) conditional(s32[]{:T(128)} %convert_element_type.152, (f32[4,128]{1,0:T(4,128)S(1)}, f32[4,128]{1,0:T(4,128)}, f32[4,128,64]{1,2,0:T(8,128)}) %tuple.61, (s32[1024]{0:T(1024)S(1)}, s32[128]{0:T(128)S(1)}, s32[]{:T(128)}, ...), branch_computations={%region_4.3_spmd, %region_5.6_spmd} | conditional | flops 176358400 | bytes 11080266 | solution.py:103
  284.6 7.0 %conditional.4 = ((f32[4,128]{1,0:T(4,128)S(1)}, f32[4,128]{1,0:T(4,128)}, f32[4,128,64]{1,2,0:T(8,128)})) conditional(s32[]{:T(128)} %convert_element_type.152, (f32[4,128]{1,0:T(4,128)S(1)}, f32[4,128]{1,0:T(4,128)}, f32[4,128,64]{1,2,0:T(8,128)}) %tuple.61, (s32[1024]{0:T(1024)S(1)}, s32[128]{0:T(128)S(1)}, s32[]{:T(128)}, ...), branch_computations={%region_4.3_spmd, %region_5.6_spmd} | conditional | flops 176358400 | bytes 11080266 | solution.py:103
  294.5 7.0 %conditional.4 = ((f32[4,128]{1,0:T(4,128)S(1)}, f32[4,128]{1,0:T(4,128)}, f32[4,128,64]{1,2,0:T(8,128)})) conditional(s32[]{:T(128)} %convert_element_type.152, (f32[4,128]{1,0:T(4,128)S(1)}, f32[4,128]{1,0:T(4,128)}, f32[4,128,64]{1,2,0:T(8,128)}) %tuple.61, (s32[1024]{0:T(1024)S(1)}, s32[128]{0:T(128)S(1)}, s32[]{:T(128)}, ...), branch_computations={%region_4.3_spmd, %region_5.6_spmd} | conditional | flops 176358400 | bytes 11080266 | solution.py:103
  304.4 6.9 %conditional.4 = ((f32[4,128]{1,0:T(4,128)S(1)}, f32[4,128]{1,0:T(4,128)}, f32[4,128,64]{1,2,0:T(8,128)})) conditional(s32[]{:T(128)} %convert_element_type.152, (f32[4,128]{1,0:T(4,128)S(1)}, f32[4,128]{1,0:T(4,128)}, f32[4,128,64]{1,2,0:T(8,128)}) %tuple.61, (s32[1024]{0:T(1024)S(1)}, s32[128]{0:T(128)S(1)}, s32[]{:T(128)}, ...), branch_computations={%region_4.3_spmd, %region_5.6_spmd} | conditional | flops 176358400 | bytes 11080266 | solution.py:103
  313.2 3.7 %all-to-all-start = ((bf16[4,32,256]{2,1,0:T(8,128)(2,1)}), bf16[4,32,256]{2,1,0:T(8,128)(2,1)S(1)}, u32[]{:S(2)}, u32[]{:S(2)}) async-start(bf16[4,32,256]{2,1,0:T(8,128)(2,1)} %convert_element_type.100), calls=%async_computation | async-start | bytes 131072 | tf_op jit(solution)/shard_map/all_to_all | solution.py:154
  319.1 3.4 %all-to-all-done = bf16[4,32,256]{2,1,0:T(8,128)(2,1)S(1)} async-done(((bf16[4,32,256]{2,1,0:T(8,128)(2,1)}), bf16[4,32,256]{2,1,0:T(8,128)(2,1)S(1)}, u32[]{:S(2)}, u32[]{:S(2)}) %all-to-all-start) | async-done | bytes 65568 | tf_op jit(solution)/shard_map/all_to_all | solution.py:154
  322.5 3.7 %convolution_convert_fusion.2 = bf16[32,2048]{1,0:T(8,128)(2,1)} fusion(bf16[32,1024]{1,0:T(8,128)(2,1)S(1)} %bitcast.57, bf16[1024,2048]{1,0:T(8,128)(2,1)} %param.27), kind=kOutput, calls=%fused_computation.29 | convolution fusion | flops 134283264 | bytes 4390912 | tf_op jit(solution)/shard_map/dot_general | solution.py:155
  (190 shorter events, 82.5 us)
Async XLA Ops:
  7.2 96.0 %copy-start = (bf16[1,256,2048]{2,1,0:T(8,128)(2,1)S(1)}, bf16[1,256,2048]{2,1,0:T(8,128)(2,1)}, u32[]{:S(2)}) copy-start(bf16[1,256,2048]{2,1,0:T(8,128)(2,1)} %param.35) | copy-start | bytes 3145732
  7.2 91.6 %all-gather.5.cloned.1.call-start = ((), (), s32[]{:S(2)}) async-start(), calls=%async_computation.5 | async-start | bytes 5242880 | tf_op jit(solution)/shard_map/all_gather | solution.py:182
  48.0 1.3 copy-start.5
  48.0 1.7 copy-start.3
  48.0 1.8 copy-start.7
  48.1 14.4 %copy-start.1 = (bf16[512,256]{1,0:T(8,128)(2,1)S(1)}, bf16[512,256]{1,0:T(8,128)(2,1)}, u32[]{:S(2)}) copy-start(bf16[512,256]{1,0:T(8,128)(2,1)} %param.26) | copy-start | bytes 786436
  48.1 14.6 %copy-start.2 = (bf16[512,256]{1,0:T(8,128)(2,1)S(1)}, bf16[512,256]{1,0:T(8,128)(2,1)}, u32[]{:S(2)}) copy-start(bf16[512,256]{1,0:T(8,128)(2,1)} %param.25) | copy-start | bytes 786436
  49.2 49.6 %copy-start.9 = (bf16[1,2048,256]{2,1,0:T(8,128)(2,1)S(1)}, bf16[1,2048,256]{2,1,0:T(8,128)(2,1)}, u32[]{:S(2)}) copy-start(bf16[1,2048,256]{2,1,0:T(8,128)(2,1)} %param.33) | copy-start | bytes 3145732
  49.2 161.1 %all-gather.3.cloned.1.call-start = ((), (), s32[]{:S(2)}) async-start(), calls=%async_computation.4 | async-start | bytes 10649600 | tf_op jit(solution)/shard_map/all_gather | solution.py:20
  63.5 39.7 %copy-start.10 = (bf16[1,2048,256]{2,1,0:T(8,128)(2,1)S(1)}, bf16[1,2048,256]{2,1,0:T(8,128)(2,1)}, u32[]{:S(2)}) copy-start(bf16[1,2048,256]{2,1,0:T(8,128)(2,1)} %param.34) | copy-start | bytes 3145732
  170.0 11.3 %copy-start.4 = (bf16[128,384]{1,0:T(8,128)(2,1)S(1)}, bf16[128,384]{1,0:T(8,128)(2,1)}, u32[]{:S(2)}) copy-start(bf16[128,384]{1,0:T(8,128)(2,1)} %param.21) | copy-start | bytes 294916
  170.0 11.6 %copy-start.6 = (f32[64,2]{0,1:T(2,128)S(1)}, f32[64,2]{0,1:T(2,128)}, u32[]{:S(2)}) copy-start(f32[64,2]{0,1:T(2,128)} %param.32) | copy-start | bytes 1540
  170.0 11.6 %copy-start.8 = (f32[64]{0:T(128)S(1)}, f32[64]{0:T(128)}, u32[]{:S(2)}) copy-start(f32[64]{0:T(128)} %param.31) | copy-start | bytes 772
  171.3 37.2 %all-to-all-start.3 = ((bf16[64,4,2048]{2,1,0:T(4,128)(2,1)}), bf16[64,4,2048]{2,1,0:T(4,128)(2,1)S(1)}, u32[]{:S(2)}, u32[]{:S(2)}) async-start(bf16[64,4,2048]{2,1,0:T(4,128)(2,1)} %reshape.212), calls=%async_computation.3 | async-start | bytes 2097152 | tf_op jit(solution)/shard_map/all_to_all | solution.py:194
  313.2 9.3 %all-to-all-start = ((bf16[4,32,256]{2,1,0:T(8,128)(2,1)}), bf16[4,32,256]{2,1,0:T(8,128)(2,1)S(1)}, u32[]{:S(2)}, u32[]{:S(2)}) async-start(bf16[4,32,256]{2,1,0:T(8,128)(2,1)} %convert_element_type.100), calls=%async_computation | async-start | bytes 131072 | tf_op jit(solution)/shard_map/all_to_all | solution.py:154
Sparse Core Ops, SparseCore 0:
  49.4 49.3 all-gather.4
  102.1 91.5 all-gather.2
where the time goes:
time: 335 us; the launch traced here: 333 us
  blocking collectives  103 us (31%)
  waiting for transfers between devices  65.2 us (19%)
  local copies, waits for them, and re-layouts  54 us (16%)
  matrix products  42 us (13%)
  other arithmetic  25.7 us (8%)
  loops' own time  15 us (4%)
  between operations  14.4 us (4%)
  starting transfers between devices  13.8 us (4%)
    all_to_all x1, blocking collectives, sent_and_summed(): lax.all_to_all(split_up(value, dim, devices), axis, 0, 0, tiled=True)  54.6 us
    all_to_all x1, blocking collectives, expert_half(): lax.all_to_all(outgoing, 'ep', split_axis=0, concat_axis=0, tiled=True)  36 us
    all_gather x1, waiting for transfers between devices, expert_half(): shard_rows = lax.all_gather(flat_rows, 'tp', axis=0, tiled=True)  35.2 us
    all_to_all x1, waiting for transfers between devices, expert_half(): lax.all_to_all(result, 'ep', split_axis=0, concat_axis=0, tiled=True)  26.5 us
    dot_general x8, matrix products, advance(): jnp.einsum('hqk,khd->hqd', raised.astype(jnp.bfloat16), values_here, pref...  18.2 us
    dynamic_slice x8, local copies, waits for them, and re-layouts, update(): lax.dynamic_slice_in_dim(value_part, row_begin, span_rows, 0)  15 us
    another operation x1, loops' own time, attend_block(): running, _ = lax.scan(update, running, jnp.arange(amount // span_rows))  14.5 us
    another operation x3, local copies, waits for them, and re-layouts  13.1 us
  transfers between devices with their start and end apart: 4, of which 3 were waited for; matrix products, arithmetic and copies ran while one was open for 7% of the time, Pallas kernels for 0%

commit v1 on v0

--- a/solution.py
+++ b/solution.py
@@ -3,11 +3,14 @@
 import jax
 import jax.numpy as jnp
 from jax import lax
+from jax.experimental import pallas as pl
+from jax.experimental.pallas import tpu as pltpu
 from jax.sharding import PartitionSpec as P
 
 NOPE = 64
 ROPE_DIM = 32
 V_DIM = 64
+GROUP = 8
 
 
 epsilon = 1e-06
@@ -54,103 +57,135 @@
     return jnp.concatenate([lower * cosine - upper * sine, lower * sine + upper * cosine], axis=-1)
 
 
-def keep_state(state_in):
-    return state_in
-
-
-def attend_block(running, query_rot, query_pos, key_part, value_part, rope_part):
-    amount = key_part.shape[0]
-    span_rows = math.gcd(amount, 1024)
-    head_count = query_rot.shape[1]
-    scale_factor = query_rot.shape[2] ** (-0.5)
-    last_query = query_pos[-1]
-
-    def update(state, block_at):
-        row_begin = block_at * span_rows
-        keys_here = lax.dynamic_slice_in_dim(key_part, row_begin, span_rows, 0).reshape(
-            span_rows, head_count, -1
+def attend(queries, kv):
+    ranks = kv.shape[0]
+    groups = ranks // GROUP
+    shift = math.log2(math.e) / math.sqrt(NOPE + ROPE_DIM)
+
+    def kernel(q_ref, kv_ref, o_ref, held, sem):
+        me = lax.axis_index("ep")
+        last = me // GROUP
+
+        def fetch(g):
+            return pltpu.make_async_copy(
+                kv_ref.at[pl.ds(g * GROUP, GROUP)], held.at[pl.ds(g * GROUP, GROUP)], sem.at[g]
+            )
+
+        for g in range(groups):
+
+            @pl.when(g <= last)
+            def _():
+                fetch(g).start()
+
+        def step(g, state, masked):
+            fetch(g).wait()
+            out = []
+            base = g * GROUP
+            rope = held[pl.ds(base, GROUP), 512:544, :].reshape(GROUP * 32, 128)
+            for p in range(2):
+                top, total, acc = state[p]
+                parts = []
+                for j in range(4):
+                    keys = held[pl.ds(base, GROUP), 128 * p + 32 * j : 128 * p + 32 * j + 32, :]
+                    both = jnp.concatenate([keys.reshape(GROUP * 32, 128), rope], axis=1)
+                    s = lax.dot_general(
+                        both, q_ref[p, j], (((1,), (1,)), ((), ())), preferred_element_type=jnp.float32
+                    )
+                    s = s.reshape(GROUP, 32, 256)
+                    if masked:
+                        rank = lax.broadcasted_iota(jnp.int32, s.shape, 0) + base
+                        row = lax.broadcasted_iota(jnp.int32, s.shape, 1) + 32 * j
+                        col = lax.broadcasted_iota(jnp.int32, s.shape, 2) & 127
+                        s = jnp.where(rank * 128 + row <= me * 128 + col, s, masked_value)
+                    parts.append(s)
+                peak = parts[0].max(axis=0)
+                for s in parts[1:]:
+                    peak = jnp.maximum(peak, s.max(axis=0))
+                peak = jnp.maximum(top, peak.max(axis=0, keepdims=True))
+                factor = jnp.exp2((top - peak) * shift)
+                summed = jnp.zeros((32, 256), jnp.float32)
+                raised = []
+                for s in parts:
+                    r = jnp.exp2((s - peak[None]) * shift)
+                    summed = summed + r.sum(axis=0)
+                    raised.append(r.astype(jnp.bfloat16))
+                total = total * factor + summed.sum(axis=0, keepdims=True)
+                acc = acc * factor
+                weights = jnp.concatenate(raised, axis=1)
+                for r in range(0, GROUP, 2):
+                    vals = jnp.concatenate(
+                        [held[base + r + i, 256 + 128 * p : 384 + 128 * p, :] for i in range(2)], axis=1
+                    )
+                    acc = acc + jnp.dot(
+                        vals, weights[r : r + 2].reshape(256, 256), preferred_element_type=jnp.float32
+                    )
+                out.append((peak, total, acc))
+            return tuple(out)
+
+        start = tuple(
+            (
+                jnp.full((1, 256), masked_value, jnp.float32),
+                jnp.zeros((1, 256), jnp.float32),
+                jnp.zeros((128, 256), jnp.float32),
+            )
+            for _ in range(2)
         )
-        values_here = lax.dynamic_slice_in_dim(value_part, row_begin, span_rows, 0).reshape(
-            span_rows, head_count, -1
-        )
-        rope_here = lax.dynamic_slice_in_dim(rope_part, row_begin, span_rows, 0)
-        key_pos = row_begin + jnp.arange(span_rows, dtype=jnp.int32)
-
-        def advance(state_in):
-            top_old, totals, weighted = state_in
-            shared = jnp.broadcast_to(
-                rope_here[:, None, :], (span_rows, head_count, rope_here.shape[1])
-            )
-            full_keys = jnp.concatenate([keys_here, shared], axis=-1)
-            scores = (
-                jnp.einsum("qhd,khd->hqk", query_rot, full_keys, preferred_element_type=jnp.float32)
-                * scale_factor
-            )
-            allowed = key_pos[None, :] <= query_pos[:, None]
-            scores = jnp.where(allowed[None], scores, masked_value)
-            top_new = jnp.maximum(top_old, jnp.max(scores, axis=-1))
-            raised = jnp.where(allowed[None], jnp.exp(scores - top_new[..., None]), 0.0)
-            factor = jnp.exp(top_old - top_new)
-            totals = totals * factor + jnp.sum(raised, axis=-1)
-            weighted = weighted * factor[..., None] + jnp.einsum(
-                "hqk,khd->hqd",
-                raised.astype(jnp.bfloat16),
-                values_here,
-                preferred_element_type=jnp.float32,
-            )
-            return (top_new, totals, weighted)
-
-        return (lax.cond(key_pos[0] <= last_query, advance, keep_state, state), None)
-
-    running, _ = lax.scan(update, running, jnp.arange(amount // span_rows))
-    return running
+        state = lax.fori_loop(0, last, lambda g, s: step(g, s, False), start)
+        state = step(last, state, True)
+        pieces = []
+        for p in range(2):
+            _, total, acc = state[p]
+            for i in range(2):
+                pieces.append(acc[64 * i : 64 * i + 64, 128 * i : 128 * i + 128] / total[:, 128 * i : 128 * i + 128])
+        o_ref[...] = jnp.concatenate(pieces, axis=0).T.astype(jnp.bfloat16)
+
+    return pl.pallas_call(
+        kernel,
+        out_shape=jax.ShapeDtypeStruct((128, 256), jnp.bfloat16),
+        in_specs=[pl.BlockSpec(memory_space=pltpu.VMEM), pl.BlockSpec(memory_space=pl.ANY)],
+        out_specs=pl.BlockSpec(memory_space=pltpu.VMEM),
+        scratch_shapes=[pltpu.VMEM(kv.shape, jnp.bfloat16), pltpu.SemaphoreType.DMA((groups,))],
+        compiler_params=pltpu.CompilerParams(vmem_limit_bytes=40 << 20),
+        name="attend",
+    )(queries, kv)
+
+
+def query_rows(query, positions):
+    rows = query.shape[0]
+    cosine, sine = tables(positions, ROPE_DIM)
+    heads = query.reshape(rows, 4, NOPE + ROPE_DIM)
+    turned = rotate(heads[..., NOPE:].astype(jnp.float32), cosine[:, None, :], sine[:, None, :])
+    turned = turned.astype(jnp.bfloat16).transpose(1, 0, 2)
+    flat = heads[..., :NOPE].transpose(1, 0, 2)
+    out = []
+    for p in range(2):
+        for j in range(4):
+            for i in range(2):
+                h = 2 * p + i
+                nope = jnp.pad(flat[h], ((0, 0), (64 * i, 64 - 64 * i)))
+                rope = jnp.pad(turned[h], ((0, 0), (32 * j, 96 - 32 * j)))
+                out.append(jnp.concatenate([nope, rope], axis=1))
+    return jnp.stack(out).reshape(2, 4, 256, 256)
 
 
 def mixer_half(query, latent, rope_key, latent_gain, key_up, value_up, out_proj):
-    query_rows = query.shape[0]
+    rows = query.shape[0]
     own_rows = latent.shape[0]
-    query_start = lax.axis_index("ep") * query_rows
+    query_start = lax.axis_index("ep") * rows
     key_start = query_start + lax.axis_index("tp") * own_rows
-    head_count = query.shape[1] // (NOPE + ROPE_DIM)
     normed = rms_scale(latent, latent_gain).astype(jnp.bfloat16)
     key_cos, key_sin = tables(key_start + jnp.arange(own_rows, dtype=jnp.int32), ROPE_DIM)
     rotated_key = rotate(rope_key.astype(jnp.float32), key_cos, key_sin).astype(jnp.bfloat16)
-    query_pos = query_start + jnp.arange(query_rows, dtype=jnp.int32)
-    query_cos, query_sin = tables(query_pos, ROPE_DIM)
-    query_heads = query.reshape(query_rows, head_count, NOPE + ROPE_DIM)
-    turned = rotate(
-        query_heads[..., NOPE:].astype(jnp.float32), query_cos[:, None, :], query_sin[:, None, :]
+    queries = query_rows(query, query_start + jnp.arange(rows, dtype=jnp.int32))
+    group_latent, group_rope = in_one_piece((normed, rotated_key), "tp", 0, 1)
+    keys = jnp.dot(group_latent, key_up, preferred_element_type=jnp.float32).astype(jnp.bfloat16)
+    values = lax.dot_general(
+        value_up, group_latent, (((0,), (1,)), ((), ())), preferred_element_type=jnp.float32
     ).astype(jnp.bfloat16)
-    query_rot = jnp.concatenate([query_heads[..., :NOPE], turned], axis=-1)
-    last_query = query_start + query_rows - 1
-    initial = (
-        jnp.full((head_count, query_rows), masked_value, jnp.float32),
-        jnp.zeros((head_count, query_rows), jnp.float32),
-        jnp.zeros((head_count, query_rows, V_DIM), jnp.float32),
-    )
-    group_latent, group_rope = in_one_piece((normed, rotated_key), "tp", 0, 1)
-    key_part = jnp.dot(group_latent, key_up, preferred_element_type=jnp.float32).astype(
-        jnp.bfloat16
-    )
-    value_part = jnp.dot(group_latent, value_up, preferred_element_type=jnp.float32).astype(
-        jnp.bfloat16
-    )
-    shard_rows = in_one_piece((key_part, value_part, group_rope), "ep", 0, 1)
-
-    def compute(state_in):
-        return attend_block(
-            state_in, query_rot, query_pos, shard_rows[0], shard_rows[1], shard_rows[2]
-        )
-
-    running = lax.cond(jnp.int32(0) <= last_query, compute, keep_state, initial)
-    totals = running[1]
-    weighted = running[2]
-    attention = (
-        (weighted / totals[..., None])
-        .transpose(1, 0, 2)
-        .reshape(query_rows, head_count * V_DIM)
-        .astype(jnp.bfloat16)
-    )
+    rope = group_rope.reshape(4, 32, 32).transpose(1, 0, 2).reshape(32, 128)
+    kv = jnp.concatenate([keys[:, :128], keys[:, 128:], values, rope], axis=0)
+    kv = lax.all_gather(kv, "ep", axis=0)
+    attention = attend(queries, kv)
     own_attention = lax.all_to_all(attention, "tp", split_axis=0, concat_axis=1, tiled=True)
     return jnp.dot(own_attention, out_proj, preferred_element_type=jnp.float32).astype(jnp.bfloat16)
 

time: 335 us -> 248 us (0.74)
  blocking collectives: 103 us -> 48.4 us
  waiting for transfers between devices: 65.2 us -> 113 us
  local copies, waits for them, and re-layouts: 54 us -> 14.6 us
  matrix products: 42 us -> 17.7 us
  other arithmetic: 25.7 us -> 8.06 us
  loops' own time: 15 us -> 0 us
  Pallas kernels: 0 us -> 13.1 us
  starting transfers between devices: 13.8 us -> 18.7 us
    all_to_all x1 -> x0, blocking collectives: 54.6 us -> none  [sent_and_summed(): lax.all_to_all(split_up(value, dim, devices), axis, 0, 0, tiled=True)]
    all_to_all x0 -> x1, waiting for transfers between devices: none -> 48.6 us  [sent_and_summed(): lax.all_to_all(split_up(value, dim, devices), axis, 0, 0, tiled=True)]
    dot_general x17 -> x1, matrix products: 23.5 us -> 0.19 us  [mixer_half(): lax.dot_general(value_up, group_latent, (((0,), (1,)), ((), ())), preferr...]
    dynamic_slice x24 -> x0, local copies, waits for them, and re-layouts: 20.4 us -> none  [the longest x8 15 us: update(): lax.dynamic_slice_in_dim(value_part, row_begin, span_rows, 0)]
    another operation x10 -> x0, loops' own time: 15 us -> none  [the longest x1 14.5 us: attend_block(): running, _ = lax.scan(update, running, jnp.arange(amount // span_rows))]
    pallas_call x0 -> x1, Pallas kernels: none -> 13.1 us  [attend(): pl.pallas_call(kernel, out_shape=jax.ShapeDtypeStruct((128, 256), jnp.bfl...]
    another operation x3, local copies, waits for them, and re-layouts: 13.1 us -> 0.71 us  [the longest x1 0.53 us: query_rows(): return jnp.stack(out).reshape(2, 4, 256, 256)]
    add x17 -> x0, other arithmetic: 10.2 us -> none  [the longest x8 10.2 us: advance(): totals = totals * factor + jnp.sum(raised, axis=-1)]
  transfers between devices with their start and end apart: 4 -> 5, of which waited for: 3 -> 4; matrix products, arithmetic and copies ran while one was open for 7% -> 11% of each run, Pallas kernels for 0% -> 0%
where the time goes in v1:
time: 248 us
  waiting for transfers between devices  113 us (46%)
  blocking collectives  48.4 us (20%)
  starting transfers between devices  18.7 us (8%)
  matrix products  17.7 us (7%)
  local copies, waits for them, and re-layouts  14.6 us (6%)
  between operations  14.5 us (6%)
  Pallas kernels  13.1 us (5%)
  other arithmetic  8.06 us (3%)
    all_to_all x1, waiting for transfers between devices, sent_and_summed(): lax.all_to_all(split_up(value, dim, devices), axis, 0, 0, tiled=True)  48.6 us
    all_to_all x1, blocking collectives, expert_half(): lax.all_to_all(outgoing, 'ep', split_axis=0, concat_axis=0, tiled=True)  36 us
    all_gather x1, waiting for transfers between devices, expert_half(): shard_rows = lax.all_gather(flat_rows, 'tp', axis=0, tiled=True)  34.7 us
    all_to_all x1, waiting for transfers between devices, expert_half(): lax.all_to_all(result, 'ep', split_axis=0, concat_axis=0, tiled=True)  25.8 us
    pallas_call x1, Pallas kernels, attend(): pl.pallas_call(kernel, out_shape=jax.ShapeDtypeStruct((128, 256), jnp.bfl...  13.1 us
    all_gather x1, blocking collectives, in_one_piece(): out, at, done = (lax.all_gather(both, axis, axis=dim, tiled=True), 0, [])  12.4 us
    all_to_all x1, starting transfers between devices, expert_half(): lax.all_to_all(result, 'ep', split_axis=0, concat_axis=0, tiled=True)  10.3 us
    dot_general x1, matrix products, lower(): return jnp.dot(hidden, w_down[0], preferred_element_type=jnp.float32)  8.45 us
  transfers between devices with their start and end apart: 5, of which 4 were waited for; matrix products, arithmetic and copies ran while one was open for 11% of the time, Pallas kernels for 0%

profile of v1, /device:TPU:224, one launch (start us, length us, event | category | flops | bytes accessed | tf_op | source)
XLA Modules:
  0.0 247.6 jit_solution(9127210149363194220)
XLA Ops:
  7.2 0.8 copy.68
  9.0 1.1 fusion.12
  10.2 1.5 convolution_convert_fusion.1
  12.1 36.0 %all_to_all.34 = bf16[64,4,2048]{2,1,0:T(4,128)(2,1)S(1)} all-to-all(bf16[64,4,2048]{2,1,0:T(4,128)(2,1)S(1)} %reshape.171), channel_id=1, replica_groups=mesh['ep'=64,'tp'=4] {'ep'}, dimensions={0} | all-to-all | bytes 2097152 | tf_op jit(solution)/shard_map/all_to_all | solution.py:214
  48.1 1.1 reshape.172
  50.0 12.4 %all_gather.12 = bf16[128,544]{1,0:T(8,128)(2,1)S(1)} all-gather(bf16[32,544]{1,0:T(8,128)(2,1)S(1)} %pad_maximum_fusion.1), channel_id=1, replica_groups=mesh['ep'=64,'tp'=4] {'tp'}, dimensions={0}, use_global_device_ids=true | all-gather | bytes 174080 | tf_op jit(solution)/shard_map/all_gather | solution.py:23
  64.0 34.7 %all-gather.4.cloned.1.call-done = bf16[1024,2048]{1,0:T(8,128)(2,1)} async-done(((bf16[256,2048]{1,0:T(8,128)(2,1)}), bf16[1024,2048]{1,0:T(8,128)(2,1)}) %all-gather.4.cloned.1.call-update) | async-done | bytes 4194320 | tf_op jit(solution)/shard_map/all_gather | solution.py:217
  98.8 3.7 %fusion.5 = f32[1024,256]{1,0:T(8,128)S(1)} fusion(bf16[1024,2048]{1,0:T(8,128)(2,1)} %all-gather.4.cloned.1.call-done, bf16[1,2048,256]{2,1,0:T(8,128)(2,1)} %param.27), kind=kOutput, calls=%fused_computation.11 | convolution fusion | flops 1073741824 | bytes 6291456 | tf_op jit(solution)/shard_map/dot_general | solution.py:218
  102.5 8.5 %convolution_convert_fusion = bf16[1024,2048]{1,0:T(8,128)(2,1)} fusion(bf16[1024,2048]{1,0:T(8,128)(2,1)} %all-gather.4.cloned.1.call-done, bf16[1,256,2048]{2,1,0:T(8,128)(2,1)S(1)} %copy-done, bf16[1,2048,256]{2,1,0:T(8,128)(2,1)S(1)} %copy-done.10, f32[1024,256]{1,0:T(8,128)S(1)} %fusion.5), kind=kOutput, calls=%fused_computation.1 | convolution fusion | flops 2151153664 | bytes 11534336 | tf_op jit(solution)/shard_map/dot_general | solution.py:223
  111.0 5.0 %all-to-all-start.2 = ((bf16[4,256,2048]{2,1,0:T(8,128)(2,1)}), bf16[4,256,2048]{2,1,0:T(8,128)(2,1)}, u32[]{:S(2)}, u32[]{:S(2)}) async-start(bf16[4,256,2048]{2,1,0:T(8,128)(2,1)} %bitcast.123), calls=%async_computation.2 | async-start | bytes 8388608 | tf_op jit(solution)/shard_map/all_to_all | solution.py:37
  116.4 48.6 %all-to-all-done.2 = bf16[4,256,2048]{2,1,0:T(8,128)(2,1)} async-done(((bf16[4,256,2048]{2,1,0:T(8,128)(2,1)}), bf16[4,256,2048]{2,1,0:T(8,128)(2,1)}, u32[]{:S(2)}, u32[]{:S(2)}) %all-to-all-start.2) | async-done | bytes 4194336 | tf_op jit(solution)/shard_map/all_to_all | solution.py:37
  165.0 3.3 %reduce_sum.66 = bf16[256,2048]{1,0:T(8,128)(2,1)S(1)} reduce(bf16[4,256,2048]{2,1,0:T(8,128)(2,1)} %all-to-all-done.2, bf16[]{:T(256)} %constant.17.clone.1), dimensions={0}, to_apply=%region_6.7 | reduce | flops 1572864 | bytes 5242882 | tf_op jit(solution)/shard_map/reduce_sum | solution.py:38
  168.3 1.2 reshape.174
  169.6 10.3 %all-to-all-start.3 = ((bf16[64,4,2048]{2,1,0:T(4,128)(2,1)}), bf16[64,4,2048]{2,1,0:T(4,128)(2,1)}, u32[]{:S(2)}, u32[]{:S(2)}) async-start(bf16[64,4,2048]{2,1,0:T(4,128)(2,1)} %reshape.174), calls=%async_computation.3 | async-start | bytes 2097152 | tf_op jit(solution)/shard_map/all_to_all | solution.py:229
  181.0 25.8 %all-to-all-done.3 = bf16[64,4,2048]{2,1,0:T(4,128)(2,1)} async-done(((bf16[64,4,2048]{2,1,0:T(4,128)(2,1)}), bf16[64,4,2048]{2,1,0:T(4,128)(2,1)}, u32[]{:S(2)}, u32[]{:S(2)}) %all-to-all-start.3) | async-done | bytes 1048608 | tf_op jit(solution)/shard_map/all_to_all | solution.py:229
  206.8 1.3 reshape.175
  208.1 1.8 gather_fusion
  209.9 1.7 reshape.176
  211.6 3.5 %copy-done.1 = bf16[34816,128]{1,0:T(8,128)(2,1)S(1)} copy-done((bf16[34816,128]{1,0:T(8,128)(2,1)S(1)}, bf16[34816,128]{1,0:T(8,128)(2,1)}, u32[]{:S(2)}) %copy-start.1) | copy-done | bytes 8912920
  215.1 13.1 %attend.1 = bf16[128,256]{1,0:T(8,128)(2,1)} custom-call(bf16[2,4,256,256]{3,2,1,0:T(8,128)(2,1)S(1)} %bitcast.122, bf16[64,544,128]{2,1,0:T(8,128)(2,1)S(1)} %bitcast.121), custom_call_target="tpu_custom_call" | custom-call | tf_op jit(solution)/shard_map/attend/pallas_call | solution.py:142
  228.2 3.3 %all-to-all-start = ((bf16[4,32,256]{2,1,0:T(8,128)(2,1)}), bf16[4,32,256]{2,1,0:T(8,128)(2,1)S(1)}, u32[]{:S(2)}, u32[]{:S(2)}) async-start(bf16[4,32,256]{2,1,0:T(8,128)(2,1)} %bitcast.33), calls=%async_computation | async-start | bytes 131072 | tf_op jit(solution)/shard_map/all_to_all | solution.py:189
  231.5 2.2 multiply_reduce_fusion
  233.8 3.4 %all-to-all-done = bf16[4,32,256]{2,1,0:T(8,128)(2,1)S(1)} async-done(((bf16[4,32,256]{2,1,0:T(8,128)(2,1)}), bf16[4,32,256]{2,1,0:T(8,128)(2,1)S(1)}, u32[]{:S(2)}, u32[]{:S(2)}) %all-to-all-start) | async-done | bytes 65568 | tf_op jit(solution)/shard_map/all_to_all | solution.py:189
  237.1 3.7 %convolution_convert_fusion.2 = bf16[32,2048]{1,0:T(8,128)(2,1)} fusion(bf16[32,1024]{1,0:T(8,128)(2,1)S(1)} %bitcast.126, bf16[1024,2048]{1,0:T(8,128)(2,1)} %param.21), kind=kOutput, calls=%fused_computation.3 | convolution fusion | flops 134283264 | bytes 4390912 | tf_op jit(solution)/shard_map/dot_general | solution.py:190
  (89 shorter events, 5.0 us)
Async XLA Ops:
  7.2 95.3 %copy-start = (bf16[1,256,2048]{2,1,0:T(8,128)(2,1)S(1)}, bf16[1,256,2048]{2,1,0:T(8,128)(2,1)}, u32[]{:S(2)}) copy-start(bf16[1,256,2048]{2,1,0:T(8,128)(2,1)} %param.29) | copy-start | bytes 3145732
  7.2 91.6 %all-gather.4.cloned.1.call-start = ((), (), s32[]{:S(2)}) async-start(), calls=%async_computation.4 | async-start | bytes 5242880 | tf_op jit(solution)/shard_map/all_gather | solution.py:217
  10.1 39.2 %copy-start.6 = (bf16[32,32]{1,0:T(8,128)(2,1)S(1)}, bf16[32,32]{1,0:T(8,128)(2,1)}, u32[]{:S(2)}) copy-start(bf16[32,32]{1,0:T(8,128)(2,1)} %param.17) | copy-start | bytes 6148
  10.1 39.6 %copy-start.4 = (bf16[32,512]{1,0:T(8,128)(2,1)S(1)}, bf16[32,512]{1,0:T(8,128)(2,1)}, u32[]{:S(2)}) copy-start(bf16[32,512]{1,0:T(8,128)(2,1)} %param.16) | copy-start | bytes 98308
  10.1 39.7 %copy-start.8 = (f32[512]{0:T(512)S(1)}, f32[512]{0:T(512)}, u32[]{:S(2)}) copy-start(f32[512]{0:T(512)} %param.18) | copy-start | bytes 6148
  11.6 50.8 %copy-start.2 = (bf16[512,256]{1,0:T(8,128)(2,1)S(1)}, bf16[512,256]{1,0:T(8,128)(2,1)}, u32[]{:S(2)}) copy-start(bf16[512,256]{1,0:T(8,128)(2,1)} %param.19) | copy-start | bytes 786436
  48.1 14.9 %copy-start.3 = (bf16[512,256]{1,0:T(8,128)(2,1)S(1)}, bf16[512,256]{1,0:T(8,128)(2,1)}, u32[]{:S(2)}) copy-start(bf16[512,256]{1,0:T(8,128)(2,1)} %param.20) | copy-start | bytes 786436
  49.2 162.4 %all-gather.6.cloned.1.call-start = ((), (), s32[]{:S(2)}) async-start(), calls=%async_computation.5 | async-start | bytes 9052160 | tf_op jit(solution)/shard_map/all_gather | solution.py:187
  63.2 39.3 %copy-start.10 = (bf16[1,2048,256]{2,1,0:T(8,128)(2,1)S(1)}, bf16[1,2048,256]{2,1,0:T(8,128)(2,1)}, u32[]{:S(2)}) copy-start(bf16[1,2048,256]{2,1,0:T(8,128)(2,1)} %param.28) | copy-start | bytes 3145732
  111.0 5.0 %copy-start.5 = (bf16[128,384]{1,0:T(8,128)(2,1)S(1)}, bf16[128,384]{1,0:T(8,128)(2,1)}, u32[]{:S(2)}) copy-start(bf16[128,384]{1,0:T(8,128)(2,1)} %param.15) | copy-start | bytes 294916
  111.0 54.0 %all-to-all-start.2 = ((bf16[4,256,2048]{2,1,0:T(8,128)(2,1)}), bf16[4,256,2048]{2,1,0:T(8,128)(2,1)}, u32[]{:S(2)}, u32[]{:S(2)}) async-start(bf16[4,256,2048]{2,1,0:T(8,128)(2,1)} %bitcast.123), calls=%async_computation.2 | async-start | bytes 8388608 | tf_op jit(solution)/shard_map/all_to_all | solution.py:37
  168.3 12.5 %copy-start.7 = (f32[64,2]{0,1:T(2,128)S(1)}, f32[64,2]{0,1:T(2,128)}, u32[]{:S(2)}) copy-start(f32[64,2]{0,1:T(2,128)} %param.26) | copy-start | bytes 1540
  168.3 12.5 %copy-start.9 = (f32[64]{0:T(128)S(1)}, f32[64]{0:T(128)}, u32[]{:S(2)}) copy-start(f32[64]{0:T(128)} %param.25) | copy-start | bytes 772
  169.6 37.2 %all-to-all-start.3 = ((bf16[64,4,2048]{2,1,0:T(4,128)(2,1)}), bf16[64,4,2048]{2,1,0:T(4,128)(2,1)}, u32[]{:S(2)}, u32[]{:S(2)}) async-start(bf16[64,4,2048]{2,1,0:T(4,128)(2,1)} %reshape.174), calls=%async_computation.3 | async-start | bytes 2097152 | tf_op jit(solution)/shard_map/all_to_all | solution.py:229
  211.6 3.5 %copy-start.1 = (bf16[34816,128]{1,0:T(8,128)(2,1)S(1)}, bf16[34816,128]{1,0:T(8,128)(2,1)}, u32[]{:S(2)}) copy-start(bf16[34816,128]{1,0:T(8,128)(2,1)} %all-gather.6.cloned.1.call-done) | copy-start | bytes 26738692
  228.2 8.9 %all-to-all-start = ((bf16[4,32,256]{2,1,0:T(8,128)(2,1)}), bf16[4,32,256]{2,1,0:T(8,128)(2,1)S(1)}, u32[]{:S(2)}, u32[]{:S(2)}) async-start(bf16[4,32,256]{2,1,0:T(8,128)(2,1)} %bitcast.33), calls=%async_computation | async-start | bytes 131072 | tf_op jit(solution)/shard_map/all_to_all | solution.py:189
Sparse Core Ops, SparseCore 0:
  49.3 49.3 all-gather.3
  102.1 87.4 all-gather.5

commit v2 on v1

--- a/solution.py
+++ b/solution.py
@@ -11,6 +11,7 @@
 ROPE_DIM = 32
 V_DIM = 64
 GROUP = 8
+MESH = pl.DeviceIdType.MESH
 
 
 epsilon = 1e-06
@@ -190,47 +191,311 @@
     return jnp.dot(own_attention, out_proj, preferred_element_type=jnp.float32).astype(jnp.bfloat16)
 
 
+def exchange(nx, where, share, w_gate, w_up, w_down):
+    width = nx.shape[1] // 4
+    units = w_gate.shape[1]
+    ranks = lax.axis_size("ep")
+    depth = ranks // 8
+    f32, bf16 = jnp.float32, jnp.bfloat16
+
+    def kernel(
+        nx_ref, where_ref, share_ref, wg_hbm, wu_hbm, wd_hbm, o_ref,
+        xn, pos, shr, slab, rows, wg, wu, wd, hid, back, ret, moved, final, mix,
+        load_sem, own_sem, small_recv, arrive, ret_sem, ring_recv, send_sem,
+    ):
+        me, t = lax.axis_index("ep"), lax.axis_index("tp")
+        z = me // 8
+        right, left = lax.rem(t + 1, 4), lax.rem(t + 3, 4)
+
+        loads = [
+            pltpu.make_async_copy(wg_hbm, wg, load_sem.at[0]),
+            pltpu.make_async_copy(wu_hbm, wu, load_sem.at[1]),
+            pltpu.make_async_copy(wd_hbm.at[:, pl.ds(pl.multiple_of(t * width, width), width)], wd.at[t], load_sem.at[2]),
+        ]
+        for c in loads:
+            c.start()
+
+        barrier = pltpu.get_barrier_semaphore()
+
+        def greet(k, _):
+            pl.semaphore_signal(barrier, inc=1, device_id=(lax.rem(me + k, ranks), t), device_id_type=MESH)
+            return 0
+
+        lax.fori_loop(1, ranks, greet, 0)
+        for k in range(1, 4):
+            pl.semaphore_signal(barrier, inc=1, device_id=(me, lax.rem(t + k, 4)), device_id_type=MESH)
+        pl.semaphore_wait(barrier, ranks + 2)
+
+        def remote(s, d, send, recv, e, x):
+            return pltpu.make_async_remote_copy(
+                src_ref=s, dst_ref=d, send_sem=send, recv_sem=recv, device_id=(e, x), device_id_type=MESH
+            )
+
+        def cols(x):
+            return pl.ds(pl.multiple_of(x * width, width), width)
+
+        def small(k, kind):
+            x = lax.rem(t + k, 4)
+            send, recv = send_sem.at[6 + 3 * kind + k - 1], small_recv.at[kind, t]
+            if kind == 0:
+                return remote(nx_ref.at[:, cols(x)], xn.at[t], send, recv, me, x)
+            if kind == 1:
+                return remote(where_ref, pos.at[t], send, recv, me, x)
+            if kind == 2:
+                return remote(share_ref, shr.at[t], send, recv, me, x)
+            if kind == 3:
+                return remote(wd_hbm.at[:, cols(x)], wd.at[t], send, recv, me, x)
+            return remote(moved.at[x], final.at[:, cols(t)], send, recv, me, x)
+
+        def small_arrived(k, kind):
+            x = lax.rem(t + k, 4)
+            recv = small_recv.at[kind, x]
+            ref = (xn.at[x], pos.at[x], shr.at[x], wd.at[x], final.at[:, cols(x)])[kind]
+            return remote(ref, ref, send_sem.at[5], recv, me, x)
+
+        for kind in range(4):
+            for k in (1, 3, 2):
+                small(k, kind).start()
+        xn[t] = nx_ref[:, cols(t)]
+        pos[t] = where_ref[...]
+        shr[t] = share_ref[...]
+        for kind in range(3):
+            for k in range(1, 4):
+                small_arrived(k, kind).wait_recv()
+
+        place = pos[0] + pos[1] + pos[2] + pos[3] - 1
+        first, second = place[0:1], place[1:2]
+        tokens = xn[...].reshape(256, width)
+
+        def offset(i):
+            half = (i + 1) // 2
+            return jnp.where(lax.rem(i, 2) == 1, depth // 2 - half, depth // 2 + half)
+
+        def own_slab():
+            return pltpu.make_async_copy(slab.at[me], rows.at[t, me], own_sem.at[0])
+
+        def dispatch(i, _):
+            zd = lax.rem(z + offset(i), depth)
+            row = lax.broadcasted_iota(jnp.int32, (128, 256), 0) + zd * 128
+            table = jnp.where((row == first) | (row == second), 1.0, 0.0).astype(bf16)
+            out = jnp.dot(table, tokens, preferred_element_type=f32).astype(bf16)
+            slab[pl.ds(zd * 8, 8)] = out.reshape(8, 16, width)
+
+            def send(k, _):
+                dst = zd * 8 + k
+
+                @pl.when(dst != me)
+                def _():
+                    remote(slab.at[dst], rows.at[t, me], send_sem.at[0], arrive.at[me], dst, t).start()
+
+                return 0
+
+            lax.fori_loop(0, 8, send, 0)
+            return 0
+
+        lax.fori_loop(0, depth, dispatch, 0)
+        own_slab().start()
+
+        def ring(kind, chunk, block, d):
+            buf = rows if kind < 2 else hid
+            to = right if d == 0 else left
+            origin = t if kind % 2 == 0 else (left if d == 0 else right)
+            part = pl.ds(block * 8, 8) if kind % 2 == 0 else pl.ds(block * 8 + 4 * d, 4)
+            ref = buf.at[origin, part]
+            return remote(ref, ref, send_sem.at[1 + kind], ring_recv.at[kind, d, chunk], me, to)
+
+        def ring_arrived(kind, chunk, block, d):
+            buf = rows if kind < 2 else hid
+            origin = (left if d == 0 else right) if kind % 2 == 0 else lax.rem(t + 2, 4)
+            part = pl.ds(block * 8, 8) if kind % 2 == 0 else pl.ds(block * 8 + 4 * d, 4)
+            ref = buf.at[origin, part]
+            return remote(ref, ref, send_sem.at[5], ring_recv.at[kind, d, chunk], me, left)
+
+        for c in loads:
+            c.wait()
+
+        def block_of(chunk):
+            return lax.rem(z - offset(chunk) + depth, depth)
+
+        def stage(s, _):
+            @pl.when(s < depth)
+            def _():
+                block = block_of(s)
+
+                def got(k, _):
+                    e = block * 8 + k
+
+                    @pl.when(e != me)
+                    def _():
+                        remote(rows.at[t, e], rows.at[t, e], send_sem.at[5], arrive.at[e], e, t).wait_recv()
+
+                    @pl.when(e == me)
+                    def _():
+                        own_slab().wait()
+
+                    return 0
+
+                lax.fori_loop(0, 8, got, 0)
+                for d in range(2):
+                    ring(0, s, block, d).start()
+
+            @pl.when((s >= 1) & (s < depth + 1))
+            def _():
+                block = block_of(s - 1)
+                for d in range(2):
+                    ring_arrived(0, s - 1, block, d).wait_recv()
+                    ring(1, s - 1, block, d).start()
+
+            @pl.when((s >= 2) & (s < depth + 2))
+            def _():
+                block = block_of(s - 2)
+                for d in range(2):
+                    ring_arrived(1, s - 2, block, d).wait_recv()
+                gate = jnp.zeros((128, units), f32)
+                up = jnp.zeros((128, units), f32)
+                for x in range(4):
+                    part = rows[x, pl.ds(block * 8, 8)].reshape(128, width)
+                    gate = gate + jnp.dot(part, wg[width * x : width * x + width], preferred_element_type=f32)
+                    up = up + jnp.dot(part, wu[width * x : width * x + width], preferred_element_type=f32)
+                hidden = (gate / (1.0 + jnp.exp(-gate)) * up).astype(bf16)
+                hid[t, pl.ds(block * 8, 8)] = hidden.reshape(8, 16, units)
+                for d in range(2):
+                    ring(2, s - 2, block, d).start()
+
+            @pl.when((s >= 3) & (s < depth + 3))
+            def _():
+                block = block_of(s - 3)
+                for d in range(2):
+                    ring_arrived(2, s - 3, block, d).wait_recv()
+                    ring(3, s - 3, block, d).start()
+
+            @pl.when(s == 4)
+            def _():
+                for k in range(1, 4):
+                    small_arrived(k, 3).wait_recv()
+
+            @pl.when(s >= 4)
+            def _():
+                block = block_of(s - 4)
+                for d in range(2):
+                    ring_arrived(3, s - 4, block, d).wait_recv()
+                total = jnp.zeros((128, width), f32)
+                for x in range(4):
+                    part = hid[x, pl.ds(block * 8, 8)].reshape(128, units)
+                    total = total + jnp.dot(part, wd[x], preferred_element_type=f32).astype(bf16).astype(f32)
+                back[pl.ds(block * 8, 8)] = total.astype(bf16).reshape(8, 16, width)
+
+                def send(k, _):
+                    e = block * 8 + k
+
+                    @pl.when(e != me)
+                    def _():
+                        remote(back.at[e], ret.at[me], send_sem.at[21], ret_sem.at[me], e, t).start()
+
+                    return 0
+
+                lax.fori_loop(0, 8, send, 0)
+
+            return 0
+
+        lax.fori_loop(0, depth + 4, stage, 0)
+
+        portion = shr[0] + shr[1] + shr[2] + shr[3]
+        high = portion.astype(bf16).astype(f32)
+        low = portion - high
+        for c in range(4):
+            row = lax.broadcasted_iota(jnp.int32, (ranks * 4, 256), 0) + c * ranks * 4
+            for n, part in enumerate((high, low)):
+                table = jnp.where(row == first, part[0:1], 0.0) + jnp.where(row == second, part[1:2], 0.0)
+                mix[n, :, c * ranks * 4 : (c + 1) * ranks * 4] = table.T.astype(bf16)
+        ret[me] = back[me]
+
+        def came(e, _):
+            @pl.when(e != me)
+            def _():
+                remote(ret.at[e], ret.at[e], send_sem.at[5], ret_sem.at[e], e, t).wait_recv()
+
+            return 0
+
+        lax.fori_loop(0, ranks, came, 0)
+        given = ret[...].reshape(ranks * 16, width)
+        summed = jnp.dot(mix[0], given, preferred_element_type=f32) + jnp.dot(
+            mix[1], given, preferred_element_type=f32
+        )
+        moved[...] = summed.astype(bf16).reshape(4, 64, width)
+        for k in (1, 3, 2):
+            small(k, 4).start()
+        final[:, cols(t)] = moved[t]
+        for k in range(1, 4):
+            small_arrived(k, 4).wait_recv()
+        o_ref[...] = final[...]
+
+        def drain(ref, sem):
+            remote(ref, ref, sem, arrive.at[0], me, left).wait_send()
+
+        drain(slab.at[pl.ds(0, ranks - 1)], send_sem.at[0])
+        drain(rows.at[pl.ds(0, 2)], send_sem.at[1])
+        drain(rows.at[0], send_sem.at[2])
+        drain(hid.at[pl.ds(0, 2)], send_sem.at[3])
+        drain(hid.at[0], send_sem.at[4])
+        drain(back.at[pl.ds(0, ranks - 1)], send_sem.at[21])
+        for kind in range(5):
+            for k in range(1, 4):
+                small(k, kind).wait_send()
+
+    vmem = pl.BlockSpec(memory_space=pltpu.VMEM)
+    hbm = pl.BlockSpec(memory_space=pl.ANY)
+    return pl.pallas_call(
+        kernel,
+        out_shape=jax.ShapeDtypeStruct(nx.shape, bf16),
+        in_specs=[vmem, vmem, vmem, hbm, hbm, hbm],
+        out_specs=vmem,
+        scratch_shapes=[
+            pltpu.VMEM((4, 64, width), bf16),
+            pltpu.VMEM((4, 8, 256), jnp.int32),
+            pltpu.VMEM((4, 8, 256), f32),
+            pltpu.VMEM((ranks, 16, width), bf16),
+            pltpu.VMEM((4, ranks, 16, width), bf16),
+            pltpu.VMEM(w_gate.shape, bf16),
+            pltpu.VMEM(w_up.shape, bf16),
+            pltpu.VMEM((4, units, width), bf16),
+            pltpu.VMEM((4, ranks, 16, units), bf16),
+            pltpu.VMEM((ranks, 16, width), bf16),
+            pltpu.VMEM((ranks, 16, width), bf16),
+            pltpu.VMEM((4, 64, width), bf16),
+            pltpu.VMEM(nx.shape, bf16),
+            pltpu.VMEM((2, 256, ranks * 16), bf16),
+            pltpu.SemaphoreType.DMA((3,)),
+            pltpu.SemaphoreType.DMA((1,)),
+            pltpu.SemaphoreType.DMA((5, 4)),
+            pltpu.SemaphoreType.DMA((ranks,)),
+            pltpu.SemaphoreType.DMA((ranks,)),
+            pltpu.SemaphoreType.DMA((4, 2, 8)),
+            pltpu.SemaphoreType.DMA((22,)),
+        ],
+        compiler_params=pltpu.CompilerParams(
+            collective_id=0, has_side_effects=True, vmem_limit_bytes=40 << 20
+        ),
+        cost_estimate=pl.CostEstimate(flops=5 * 10**9, bytes_accessed=3 * 10**7, transcendentals=0),
+        name="exchange",
+    )(nx, where, share, w_gate, w_up, w_down)
+
+
 def expert_half(tokens, moe_gain, routes, group_prob, expert_prob, w_gate, w_up, w_down):
-    row_count, model_width = tokens.shape
-    top_count = routes.shape[1]
+    row_count = tokens.shape[0]
     expert_count = lax.axis_size("ep")
-    capacity = 2 * top_count * row_count // expert_count
-    normed = rms_scale(tokens, moe_gain).astype(jnp.bfloat16)
-    flat_routes = routes.reshape(-1)
-    onehot = (flat_routes[:, None] == jnp.arange(expert_count, dtype=jnp.int32)[None, :]).astype(
-        jnp.int32
-    )
+    nx = rms_scale(tokens, moe_gain).astype(jnp.bfloat16)
+    flat = routes.reshape(-1)
+    onehot = (flat[:, None] == jnp.arange(expert_count, dtype=jnp.int32)[None, :]).astype(jnp.int32)
     earlier = jnp.cumsum(onehot, axis=0) - onehot
-    slot_index = jnp.sum(earlier * onehot, axis=1)
-    target = flat_routes * capacity + slot_index
-    owner = target[None, :] == jnp.arange(expert_count * capacity, dtype=jnp.int32)[:, None]
-    dispatch_table = jnp.any(
-        owner.reshape(expert_count * capacity, row_count, top_count), axis=2
-    ).astype(jnp.bfloat16)
-    outgoing = jnp.dot(dispatch_table, normed, preferred_element_type=jnp.float32).astype(
-        jnp.bfloat16
-    )
-    outgoing = outgoing.reshape(expert_count, capacity, model_width)
-    arrived = lax.all_to_all(outgoing, "ep", split_axis=0, concat_axis=0, tiled=True)
-    sources, slots, _ = arrived.shape
-    flat_rows = arrived.reshape(sources * slots, model_width)
-    shard_rows = lax.all_gather(flat_rows, "tp", axis=0, tiled=True)
-    gate_values = jnp.dot(shard_rows, w_gate[0], preferred_element_type=jnp.float32)
-    up_values = jnp.dot(shard_rows, w_up[0], preferred_element_type=jnp.float32)
-    hidden = (jax.nn.silu(gate_values) * up_values).astype(jnp.bfloat16)
-
-    def lower(offset, amount):
-        return jnp.dot(hidden, w_down[0], preferred_element_type=jnp.float32)
-
-    summed = sent_and_summed(
-        lower(jnp.int32(0), sources * slots * lax.axis_size("tp")).astype(jnp.bfloat16), "tp", 0
-    )
-    result = summed.astype(jnp.bfloat16).reshape(sources, slots, model_width)
-    returned = lax.all_to_all(result, "ep", split_axis=0, concat_axis=0, tiled=True)
-    returned_flat = returned.reshape(expert_count * capacity, model_width)
-    picked = returned_flat[target].reshape(row_count, top_count, model_width).astype(jnp.float32)
-    shares = group_prob[:, None] * expert_prob / jnp.sum(expert_prob, axis=1, keepdims=True)
-    return jnp.sum(shares[:, :, None] * picked, axis=1).astype(jnp.bfloat16)
+    slot = jnp.sum(earlier * onehot, axis=1)
+    t = lax.axis_index("tp")
+    target = (flat * 16 + t * 4 + slot + 1).reshape(row_count, 2).T
+    shares = (group_prob[:, None] * expert_prob / jnp.sum(expert_prob, axis=1, keepdims=True)).T
+    mine = (jnp.arange(256, dtype=jnp.int32) // 64 == t)[None, :]
+    where = jnp.pad(jnp.where(mine, jnp.tile(target, (1, 4)), 0), ((0, 6), (0, 0)))
+    share = jnp.pad(jnp.where(mine, jnp.tile(shares, (1, 4)), 0.0), ((0, 6), (0, 0)))
+    return exchange(nx, where, share, w_gate[0], w_up[0], w_down[0])
 
 
 def body(

time: 248 us -> 245 us (0.988)
  the two profiles are of different devices: /device:TPU:224 before, /device:TPU:1 now
where the time goes in v2:
time: 245 us; the launch traced here: 244 us
  Pallas kernels  111 us (45%)
  waiting for transfers between devices  85.7 us (35%)
  between operations  14.4 us (6%)
  local copies, waits for them, and re-layouts  11.1 us (5%)
  blocking collectives  10.4 us (4%)
  matrix products  5 us (2%)
  starting transfers between devices  4.02 us (2%)
  other arithmetic  3.15 us (1%)
    pallas_call x1, Pallas kernels, exchange(): pl.pallas_call(kernel, out_shape=jax.ShapeDtypeStruct(nx.shape, bf16), in...  108 us
    all_gather x1, waiting for transfers between devices, mixer_half(): kv = lax.all_gather(kv, 'ep', axis=0)  85.7 us
    all_gather x1, blocking collectives, in_one_piece(): out, at, done = (lax.all_gather(both, axis, axis=dim, tiled=True), 0, [])  10.4 us
    unnamed x24, local copies, waits for them, and re-layouts  8.67 us
  transfers between devices with their start and end apart: 2, of which 1 were waited for; matrix products, arithmetic and copies ran while one was open for 1% of the time, Pallas kernels for 44%

profile of v2, /device:TPU:1, one launch (start us, length us, event | category | flops | bytes accessed | tf_op | source)
XLA Modules:
  0.0 244.4 jit_solution(4374916926273373169)
XLA Ops:
  7.3 0.9 copy.54
  8.5 0.9 fusion.26
  9.4 0.8 fusion.28
  10.3 10.4 %all_gather.9 = bf16[128,544]{1,0:T(8,128)(2,1)S(1)} all-gather(bf16[32,544]{1,0:T(8,128)(2,1)S(1)} %pad_maximum_fusion.1), channel_id=1, replica_groups=mesh['ep'=64,'tp'=4] {'tp'}, dimensions={0}, use_global_device_ids=true | all-gather | bytes 174080 | tf_op jit(solution)/shard_map/all_gather | solution.py:24
  20.7 0.2 convolution_convert_fusion.2
  21.2 1.1 fusion
  22.4 0.8 copy.60
  23.2 1.0 copy.52
  24.8 0.5 copy.53
  25.4 0.1 eq.27
  25.6 0.2 reduce_window_sum.11
  25.8 0.2 select_reduce_fusion
  26.0 0.1 reduce_sum.41
  26.5 0.2 fusion.1
  26.7 0.1 fusion.3.nx_ref
  26.8 85.7 %all-gather.3.cloned.1.call-done = bf16[34816,128]{1,0:T(8,128)(2,1)} async-done(((bf16[544,128]{1,0:T(8,128)(2,1)}), bf16[34816,128]{1,0:T(8,128)(2,1)}) %all-gather.3.cloned.1.call-update) | async-done | bytes 8912912 | tf_op jit(solution)/shard_map/all_gather | solution.py:188
  112.5 3.5 %copy-done.1 = bf16[34816,128]{1,0:T(8,128)(2,1)S(1)} copy-done((bf16[34816,128]{1,0:T(8,128)(2,1)S(1)}, bf16[34816,128]{1,0:T(8,128)(2,1)}, u32[]{:S(2)}) %copy-start.1) | copy-done | bytes 8912920
  116.0 2.3 attend.1
  118.3 4.0 %all-to-all-start = ((bf16[4,32,256]{2,1,0:T(8,128)(2,1)}), bf16[4,32,256]{2,1,0:T(8,128)(2,1)S(1)}, u32[]{:S(2)}, u32[]{:S(2)}) async-start(bf16[4,32,256]{2,1,0:T(8,128)(2,1)} %bitcast.33), calls=%async_computation | async-start | bytes 131072 | tf_op jit(solution)/shard_map/all_to_all | solution.py:190
  122.3 1.2 copy-done.3
  123.5 1.2 copy-done.4
  124.7 108.4 %exchange.1 = bf16[64,2048]{1,0:T(8,128)(2,1)S(1)} custom-call(bf16[64,2048]{1,0:T(8,128)(2,1)S(1)} %fusion.3.nx_ref, s32[8,256]{1,0:T(8,128)S(1)} %pad.106.where_ref, f32[8,256]{1,0:T(8,128)S(1)} %pad.107.share_ref, bf16[2048,256]{1,0:T(8,128)(2,1)S(1)} %bitcast.110, bf16[2048,256]{1,0:T(8,128)(2,1)S(1)} %bitcast.111, bf16[256,2048]{1,0:T(8,128)(2,1)S(1)} %bitcast.112), custom_call_target="tpu_custom_call" | custom-call | flops 5000000000 | bytes 30000000 | tf_op jit(solution)/shard_map/exchange/pallas_call | solution.py:448
  233.2 3.7 %convolution_convert_fusion = bf16[32,2048]{1,0:T(8,128)(2,1)} fusion(bf16[32,1024]{1,0:T(8,128)(2,1)S(1)} %bitcast.115, bf16[1024,2048]{1,0:T(8,128)(2,1)} %param.21), kind=kOutput, calls=%fused_computation | convolution fusion | flops 134283264 | bytes 4390912 | tf_op jit(solution)/shard_map/dot_general | solution.py:191
  236.9 0.7 copy.81
  (75 shorter events, 1.8 us)
Async XLA Ops:
  7.2 13.5 %copy-start = (bf16[512,256]{1,0:T(8,128)(2,1)S(1)}, bf16[512,256]{1,0:T(8,128)(2,1)}, u32[]{:S(2)}) copy-start(bf16[512,256]{1,0:T(8,128)(2,1)} %param.19) | copy-start | bytes 786436
  7.2 18.1 %copy-start.7 = (s32[64,2]{0,1:T(2,128)S(1)}, s32[64,2]{0,1:T(2,128)}, u32[]{:S(2)}) copy-start(s32[64,2]{0,1:T(2,128)} %param.24) | copy-start | bytes 1540
  7.2 19.2 %copy-start.8 = (f32[64,2]{0,1:T(2,128)S(1)}, f32[64,2]{0,1:T(2,128)}, u32[]{:S(2)}) copy-start(f32[64,2]{0,1:T(2,128)} %param.26) | copy-start | bytes 1540
  7.2 19.2 %copy-start.9 = (f32[64]{0:T(128)S(1)}, f32[64]{0:T(128)}, u32[]{:S(2)}) copy-start(f32[64]{0:T(128)} %param.25) | copy-start | bytes 772
  7.2 19.3 %copy-start.5 = (bf16[64,2048]{1,0:T(8,128)(2,1)S(1)}, bf16[64,2048]{1,0:T(8,128)(2,1)}, u32[]{:S(2)}) copy-start(bf16[64,2048]{1,0:T(8,128)(2,1)} %param.22) | copy-start | bytes 786436
  7.2 19.5 %copy-start.6 = (f32[2048]{0:T(1024)S(1)}, f32[2048]{0:T(1024)}, u32[]{:S(2)}) copy-start(f32[2048]{0:T(1024)} %param.23) | copy-start | bytes 24580
  7.2 105.3 %all-gather.3.cloned.1.call-start = ((), (), s32[]{:S(2)}) async-start(), calls=%async_computation.1 | async-start | bytes 9052160 | tf_op jit(solution)/shard_map/all_gather | solution.py:188
  112.5 3.5 %copy-start.1 = (bf16[34816,128]{1,0:T(8,128)(2,1)S(1)}, bf16[34816,128]{1,0:T(8,128)(2,1)}, u32[]{:S(2)}) copy-start(bf16[34816,128]{1,0:T(8,128)(2,1)} %all-gather.3.cloned.1.call-done) | copy-start | bytes 26738692
  116.0 6.3 %copy-start.2 = (bf16[1,2048,256]{2,1,0:T(8,128)(2,1)S(1)}, bf16[1,2048,256]{2,1,0:T(8,128)(2,1)}, u32[]{:S(2)}) copy-start(bf16[1,2048,256]{2,1,0:T(8,128)(2,1)} %param.27) | copy-start | bytes 3145732
  118.3 114.9 %all-to-all-start = ((bf16[4,32,256]{2,1,0:T(8,128)(2,1)}), bf16[4,32,256]{2,1,0:T(8,128)(2,1)S(1)}, u32[]{:S(2)}, u32[]{:S(2)}) async-start(bf16[4,32,256]{2,1,0:T(8,128)(2,1)} %bitcast.33), calls=%async_computation | async-start | bytes 131072 | tf_op jit(solution)/shard_map/all_to_all | solution.py:190
  122.3 1.2 copy-start.3
  123.5 1.2 copy-start.4
Sparse Core Ops, SparseCore 0:
  23.3 89.1 all-gather.2

commit v3 on v2

--- a/solution.py
+++ b/solution.py
@@ -9,34 +9,12 @@
 
 NOPE = 64
 ROPE_DIM = 32
-V_DIM = 64
-GROUP = 8
 MESH = pl.DeviceIdType.MESH
 
 
 epsilon = 1e-06
 rope_base = 10000.0
 masked_value = -1e30
-
-
-def in_one_piece(arrays, axis, dim, along):
-    both = jnp.concatenate(arrays, axis=along)
-    out, at, done = (lax.all_gather(both, axis, axis=dim, tiled=True), 0, [])
-    for a in arrays:
-        done.append(lax.slice_in_dim(out, at, at + a.shape[along], axis=along))
-        at += a.shape[along]
-    return tuple(done)
-
-
-def split_up(value, dim, devices):
-    before, after = (value.shape[:dim], value.shape[dim + 1 :])
-    return jnp.moveaxis(value.reshape(*before, devices, -1, *after), dim, 0)
-
-
-def sent_and_summed(value, axis, dim):
-    devices = lax.axis_size(axis)
-    parts = lax.all_to_all(split_up(value, dim, devices), axis, 0, 0, tiled=True)
-    return jnp.sum(parts.astype(jnp.float32), axis=0)
 
 
 def rms_scale(values, gain):
@@ -56,99 +34,6 @@
     lower = values[..., :half_width]
     upper = values[..., half_width:]
     return jnp.concatenate([lower * cosine - upper * sine, lower * sine + upper * cosine], axis=-1)
-
-
-def attend(queries, kv):
-    ranks = kv.shape[0]
-    groups = ranks // GROUP
-    shift = math.log2(math.e) / math.sqrt(NOPE + ROPE_DIM)
-
-    def kernel(q_ref, kv_ref, o_ref, held, sem):
-        me = lax.axis_index("ep")
-        last = me // GROUP
-
-        def fetch(g):
-            return pltpu.make_async_copy(
-                kv_ref.at[pl.ds(g * GROUP, GROUP)], held.at[pl.ds(g * GROUP, GROUP)], sem.at[g]
-            )
-
-        for g in range(groups):
-
-            @pl.when(g <= last)
-            def _():
-                fetch(g).start()
-
-        def step(g, state, masked):
-            fetch(g).wait()
-            out = []
-            base = g * GROUP
-            rope = held[pl.ds(base, GROUP), 512:544, :].reshape(GROUP * 32, 128)
-            for p in range(2):
-                top, total, acc = state[p]
-                parts = []
-                for j in range(4):
-                    keys = held[pl.ds(base, GROUP), 128 * p + 32 * j : 128 * p + 32 * j + 32, :]
-                    both = jnp.concatenate([keys.reshape(GROUP * 32, 128), rope], axis=1)
-                    s = lax.dot_general(
-                        both, q_ref[p, j], (((1,), (1,)), ((), ())), preferred_element_type=jnp.float32
-                    )
-                    s = s.reshape(GROUP, 32, 256)
-                    if masked:
-                        rank = lax.broadcasted_iota(jnp.int32, s.shape, 0) + base
-                        row = lax.broadcasted_iota(jnp.int32, s.shape, 1) + 32 * j
-                        col = lax.broadcasted_iota(jnp.int32, s.shape, 2) & 127
-                        s = jnp.where(rank * 128 + row <= me * 128 + col, s, masked_value)
-                    parts.append(s)
-                peak = parts[0].max(axis=0)
-                for s in parts[1:]:
-                    peak = jnp.maximum(peak, s.max(axis=0))
-                peak = jnp.maximum(top, peak.max(axis=0, keepdims=True))
-                factor = jnp.exp2((top - peak) * shift)
-                summed = jnp.zeros((32, 256), jnp.float32)
-                raised = []
-                for s in parts:
-                    r = jnp.exp2((s - peak[None]) * shift)
-                    summed = summed + r.sum(axis=0)
-                    raised.append(r.astype(jnp.bfloat16))
-                total = total * factor + summed.sum(axis=0, keepdims=True)
-                acc = acc * factor
-                weights = jnp.concatenate(raised, axis=1)
-                for r in range(0, GROUP, 2):
-                    vals = jnp.concatenate(
-                        [held[base + r + i, 256 + 128 * p : 384 + 128 * p, :] for i in range(2)], axis=1
-                    )
-                    acc = acc + jnp.dot(
-                        vals, weights[r : r + 2].reshape(256, 256), preferred_element_type=jnp.float32
-                    )
-                out.append((peak, total, acc))
-            return tuple(out)
-
-        start = tuple(
-            (
-                jnp.full((1, 256), masked_value, jnp.float32),
-                jnp.zeros((1, 256), jnp.float32),
-                jnp.zeros((128, 256), jnp.float32),
-            )
-            for _ in range(2)
-        )
-        state = lax.fori_loop(0, last, lambda g, s: step(g, s, False), start)
-        state = step(last, state, True)
-        pieces = []
-        for p in range(2):
-            _, total, acc = state[p]
-            for i in range(2):
-                pieces.append(acc[64 * i : 64 * i + 64, 128 * i : 128 * i + 128] / total[:, 128 * i : 128 * i + 128])
-        o_ref[...] = jnp.concatenate(pieces, axis=0).T.astype(jnp.bfloat16)
-
-    return pl.pallas_call(
-        kernel,
-        out_shape=jax.ShapeDtypeStruct((128, 256), jnp.bfloat16),
-        in_specs=[pl.BlockSpec(memory_space=pltpu.VMEM), pl.BlockSpec(memory_space=pl.ANY)],
-        out_specs=pl.BlockSpec(memory_space=pltpu.VMEM),
-        scratch_shapes=[pltpu.VMEM(kv.shape, jnp.bfloat16), pltpu.SemaphoreType.DMA((groups,))],
-        compiler_params=pltpu.CompilerParams(vmem_limit_bytes=40 << 20),
-        name="attend",
-    )(queries, kv)
 
 
 def query_rows(query, positions):
@@ -169,51 +54,53 @@
     return jnp.stack(out).reshape(2, 4, 256, 256)
 
 
-def mixer_half(query, latent, rope_key, latent_gain, key_up, value_up, out_proj):
+def mixer_inputs(query, latent, rope_key, latent_gain):
     rows = query.shape[0]
     own_rows = latent.shape[0]
+    t = lax.axis_index("tp")
     query_start = lax.axis_index("ep") * rows
-    key_start = query_start + lax.axis_index("tp") * own_rows
+    key_start = query_start + t * own_rows
     normed = rms_scale(latent, latent_gain).astype(jnp.bfloat16)
     key_cos, key_sin = tables(key_start + jnp.arange(own_rows, dtype=jnp.int32), ROPE_DIM)
-    rotated_key = rotate(rope_key.astype(jnp.float32), key_cos, key_sin).astype(jnp.bfloat16)
+    rotated = rotate(rope_key.astype(jnp.float32), key_cos, key_sin)
+    mine = (jnp.arange(128, dtype=jnp.int32) // 32 == t)[None, :]
+    packed = jnp.where(mine, jnp.tile(rotated, (1, 4)), 0.0).astype(jnp.bfloat16)
     queries = query_rows(query, query_start + jnp.arange(rows, dtype=jnp.int32))
-    group_latent, group_rope = in_one_piece((normed, rotated_key), "tp", 0, 1)
-    keys = jnp.dot(group_latent, key_up, preferred_element_type=jnp.float32).astype(jnp.bfloat16)
-    values = lax.dot_general(
-        value_up, group_latent, (((0,), (1,)), ((), ())), preferred_element_type=jnp.float32
-    ).astype(jnp.bfloat16)
-    rope = group_rope.reshape(4, 32, 32).transpose(1, 0, 2).reshape(32, 128)
-    kv = jnp.concatenate([keys[:, :128], keys[:, 128:], values, rope], axis=0)
-    kv = lax.all_gather(kv, "ep", axis=0)
-    attention = attend(queries, kv)
-    own_attention = lax.all_to_all(attention, "tp", split_axis=0, concat_axis=1, tiled=True)
-    return jnp.dot(own_attention, out_proj, preferred_element_type=jnp.float32).astype(jnp.bfloat16)
-
-
-def exchange(nx, where, share, w_gate, w_up, w_down):
+    return queries, jnp.concatenate([normed, packed], axis=1)
+
+
+def exchange(nx, where, share, latents, queries, w_gate, w_up, w_down, key_up, value_up, out_proj):
     width = nx.shape[1] // 4
     units = w_gate.shape[1]
     ranks = lax.axis_size("ep")
     depth = ranks // 8
     f32, bf16 = jnp.float32, jnp.bfloat16
+    shift = math.log2(math.e) / math.sqrt(NOPE + ROPE_DIM)
 
     def kernel(
-        nx_ref, where_ref, share_ref, wg_hbm, wu_hbm, wd_hbm, o_ref,
+        nx_ref, where_ref, share_ref, lat_ref, q_ref, wg_hbm, wu_hbm, wd_hbm, ku_hbm, vu_hbm, wp_hbm, mixed_ref, o_ref,
         xn, pos, shr, slab, rows, wg, wu, wd, hid, back, ret, moved, final, mix,
-        load_sem, own_sem, small_recv, arrive, ret_sem, ring_recv, send_sem,
+        lat, ku, vu, wp, kv, top, total, acc, attm, attx,
+        load_sem, own_sem, small_recv, arrive, ret_sem, ring_recv, send_sem, kv_recv, kv_send,
     ):
         me, t = lax.axis_index("ep"), lax.axis_index("tp")
         z = me // 8
+        y, c = lax.rem(me, 8) // 2, lax.rem(me, 2)
+        g0 = lax.rem(me, 8)
         right, left = lax.rem(t + 1, 4), lax.rem(t + 3, 4)
 
         loads = [
             pltpu.make_async_copy(wg_hbm, wg, load_sem.at[0]),
             pltpu.make_async_copy(wu_hbm, wu, load_sem.at[1]),
             pltpu.make_async_copy(wd_hbm.at[:, pl.ds(pl.multiple_of(t * width, width), width)], wd.at[t], load_sem.at[2]),
+            pltpu.make_async_copy(wp_hbm, wp, load_sem.at[3]),
         ]
-        for c in loads:
-            c.start()
+        early = [
+            pltpu.make_async_copy(ku_hbm, ku, load_sem.at[4]),
+            pltpu.make_async_copy(vu_hbm, vu, load_sem.at[5]),
+        ]
+        for load in early + loads:
+            load.start()
 
         barrier = pltpu.get_barrier_semaphore()
 
@@ -245,21 +132,26 @@
                 return remote(share_ref, shr.at[t], send, recv, me, x)
             if kind == 3:
                 return remote(wd_hbm.at[:, cols(x)], wd.at[t], send, recv, me, x)
-            return remote(moved.at[x], final.at[:, cols(t)], send, recv, me, x)
+            if kind == 4:
+                return remote(moved.at[x], final.at[:, cols(t)], send, recv, me, x)
+            if kind == 5:
+                return remote(lat_ref, lat.at[t], send, recv, me, x)
+            return remote(attm.at[x], attx.at[t], send, recv, me, x)
 
         def small_arrived(k, kind):
             x = lax.rem(t + k, 4)
             recv = small_recv.at[kind, x]
-            ref = (xn.at[x], pos.at[x], shr.at[x], wd.at[x], final.at[:, cols(x)])[kind]
+            ref = (xn.at[x], pos.at[x], shr.at[x], wd.at[x], final.at[:, cols(x)], lat.at[x], attx.at[x])[kind]
             return remote(ref, ref, send_sem.at[5], recv, me, x)
 
-        for kind in range(4):
+        for kind in (0, 1, 5, 2, 3):
             for k in (1, 3, 2):
                 small(k, kind).start()
+        lat[t] = lat_ref[...]
         xn[t] = nx_ref[:, cols(t)]
         pos[t] = where_ref[...]
         shr[t] = share_ref[...]
-        for kind in range(3):
+        for kind in range(2):
             for k in range(1, 4):
                 small_arrived(k, kind).wait_recv()
 
@@ -293,8 +185,118 @@
             lax.fori_loop(0, 8, send, 0)
             return 0
 
-        lax.fori_loop(0, depth, dispatch, 0)
+        def plane(dz):
+            return lax.rem(z + dz + depth, depth)
+
+        def column(dy, flip=0):
+            return lax.rem(y + dy + 4, 4) * 2 + (c if flip == 0 else 1 - c)
+
+        def along_z(d, step, arrived=False):
+            sign = 1 if d == 0 else -1
+            block = plane(-sign * (step if arrived else step - 1))
+            ref = kv.at[g0, block] if step < 4 else kv.at[g0, block, pl.ds(272 * d, 272)]
+            n = 4 * d + step - 1
+            return remote(ref, ref, kv_send.at[n], kv_recv.at[n], plane(sign) * 8 + g0, t)
+
+        def along_y(d, stage, arrived=False):
+            sign = 1 if d == 0 else -1
+            hops = stage + (1 if arrived else 0)
+            col = column(-sign * hops)
+            ref = kv.at[col] if stage == 0 else kv.at[col, pl.ds(4 * d, 4)]
+            n = 8 + 2 * stage + d
+            return remote(ref, ref, kv_send.at[n], kv_recv.at[n], z * 8 + column(sign), t)
+
+        def across(i, arrived=False):
+            ref = kv.at[column((0, -1, 1, 2)[i], 1 if arrived else 0)]
+            return remote(ref, ref, kv_send.at[12 + i], kv_recv.at[12 + i], z * 8 + column(0, 1), t)
+
+        dispatch(0, 0)
+        for k in range(1, 4):
+            small_arrived(k, 5).wait_recv()
+        for load in early:
+            load.wait()
+        flat = lat[...].reshape(128, lat.shape[2])
+        latent = flat[:, : ku.shape[0]]
+        keys = jnp.dot(latent, ku[...], preferred_element_type=f32).astype(bf16)
+        values = jnp.dot(latent, vu[...], preferred_element_type=f32)
+        kv[g0, z, 0:128] = keys[:, :128]
+        kv[g0, z, 128:256] = keys[:, 128:]
+        kv[g0, z, 256:512] = values.T.astype(bf16)
+        packed = lat[0, :, ku.shape[0] :].astype(f32)
+        for x in range(1, 4):
+            packed = packed + lat[x, :, ku.shape[0] :].astype(f32)
+        kv[g0, z, 512:544] = packed.astype(bf16)
+        for d in range(2):
+            along_z(d, 1).start()
+        for step in range(1, 4):
+            lax.fori_loop(2 * step - 1, 2 * step + 1, dispatch, 0)
+            for d in range(2):
+                along_z(d, step, True).wait_recv()
+                along_z(d, step + 1).start()
+        dispatch(depth - 1, 0)
         own_slab().start()
+        for k in range(1, 4):
+            small_arrived(k, 2).wait_recv()
+        top[...] = jnp.full(top.shape, masked_value, f32)
+        total[...] = jnp.zeros(total.shape, f32)
+        acc[...] = jnp.zeros(acc.shape, f32)
+
+        def attend(k, _):
+            for i, at in enumerate((1, 4, 5, 7)):
+
+                @pl.when(k == at)
+                def _():
+                    across(i, True).wait_recv()
+
+            dy = jnp.where(k < 2, 0, jnp.where(k >= 6, 2, jnp.where(lax.rem(k, 2) == 0, 3, 1)))
+            flip = (k == 1) | (k == 4) | (k == 5) | (k == 7)
+            col = lax.rem(y + dy, 4) * 2 + jnp.where(flip, 1 - c, c)
+            rope = kv[col, :, 512:544, :].reshape(256, 128)
+            for p in range(2):
+                parts = []
+                for j in range(4):
+                    some = kv[col, :, 128 * p + 32 * j : 128 * p + 32 * j + 32, :]
+                    both = jnp.concatenate([some.reshape(256, 128), rope], axis=1)
+                    s = lax.dot_general(both, q_ref[p, j], (((1,), (1,)), ((), ())), preferred_element_type=f32)
+                    s = s.reshape(8, 32, 256)
+                    place = lax.broadcasted_iota(jnp.int32, s.shape, 0) * 1024 + lax.broadcasted_iota(jnp.int32, s.shape, 1)
+                    query = lax.broadcasted_iota(jnp.int32, s.shape, 2) & 127
+                    parts.append(jnp.where(place - query <= (me - col) * 128 - 32 * j, s, masked_value))
+                peak = parts[0].max(axis=0)
+                for s in parts[1:]:
+                    peak = jnp.maximum(peak, s.max(axis=0))
+                before = top[p]
+                peak = jnp.maximum(before, peak.max(axis=0, keepdims=True))
+                factor = jnp.exp2((before - peak) * shift)
+                added = jnp.zeros((32, 256), f32)
+                raised = []
+                for s in parts:
+                    r = jnp.exp2((s - peak[None]) * shift)
+                    added = added + r.sum(axis=0)
+                    raised.append(r.astype(bf16))
+                total[p] = total[p] * factor + added.sum(axis=0, keepdims=True)
+                top[p] = peak
+                weights = jnp.concatenate(raised, axis=1)
+                update = acc[p] * factor
+                for r in range(0, 8, 2):
+                    vals = jnp.concatenate(
+                        [kv[col, r + i, 256 + 128 * p : 384 + 128 * p, :] for i in range(2)], axis=1
+                    )
+                    update = update + jnp.dot(vals, weights[r : r + 2].reshape(256, 256), preferred_element_type=f32)
+                acc[p] = update
+            return 0
+
+        def attended():
+            pieces = []
+            for p in range(2):
+                a, l = acc[p], total[p]
+                for i in range(2):
+                    lanes = slice(128 * i, 128 * i + 128)
+                    pieces.append(a[64 * i : 64 * i + 64, lanes] / l[:, lanes])
+            attm[...] = jnp.concatenate(pieces, axis=0).T.astype(bf16).reshape(4, 32, 256)
+            for k in (1, 3, 2):
+                small(k, 6).start()
+            attx[t] = attm[t]
 
         def ring(kind, chunk, block, d):
             buf = rows if kind < 2 else hid
@@ -311,13 +313,27 @@
             ref = buf.at[origin, part]
             return remote(ref, ref, send_sem.at[5], ring_recv.at[kind, d, chunk], me, left)
 
-        for c in loads:
-            c.wait()
+        for load in loads:
+            load.wait()
 
         def block_of(chunk):
             return lax.rem(z - offset(chunk) + depth, depth)
 
+        def pick(s, table):
+            out = jnp.int32(0)
+            for at, value in table:
+                out = jnp.where(s == at, value, out)
+            return out
+
         def stage(s, _):
+            @pl.when(s == 1)
+            def _():
+                for d in range(2):
+                    along_z(d, 4, True).wait_recv()
+                for d in range(2):
+                    along_y(d, 0).start()
+                across(0).start()
+
             @pl.when(s < depth)
             def _():
                 block = block_of(s)
@@ -390,11 +406,32 @@
 
                     @pl.when(e != me)
                     def _():
-                        remote(back.at[e], ret.at[me], send_sem.at[21], ret_sem.at[me], e, t).start()
+                        remote(back.at[e], ret.at[me], send_sem.at[27], ret_sem.at[me], e, t).start()
 
                     return 0
 
                 lax.fori_loop(0, 8, send, 0)
+
+            @pl.when(s == 7)
+            def _():
+                for d in range(2):
+                    along_y(d, 0, True).wait_recv()
+                    along_y(d, 1).start()
+                    across(1 + d).start()
+
+            @pl.when(s == 10)
+            def _():
+                for d in range(2):
+                    along_y(d, 1, True).wait_recv()
+                across(3).start()
+
+            lo = pick(s, ((3, 1), (8, 2), (9, 4), (10, 6), (11, 7)))
+            hi = pick(s, ((2, 1), (3, 2), (8, 4), (9, 6), (10, 7), (11, 8)))
+            lax.fori_loop(lo, hi, attend, 0)
+
+            @pl.when(s == 11)
+            def _():
+                attended()
 
             return 0
 
@@ -403,11 +440,11 @@
         portion = shr[0] + shr[1] + shr[2] + shr[3]
         high = portion.astype(bf16).astype(f32)
         low = portion - high
-        for c in range(4):
-            row = lax.broadcasted_iota(jnp.int32, (ranks * 4, 256), 0) + c * ranks * 4
+        for n4 in range(4):
+            row = lax.broadcasted_iota(jnp.int32, (ranks * 4, 256), 0) + n4 * ranks * 4
             for n, part in enumerate((high, low)):
                 table = jnp.where(row == first, part[0:1], 0.0) + jnp.where(row == second, part[1:2], 0.0)
-                mix[n, :, c * ranks * 4 : (c + 1) * ranks * 4] = table.T.astype(bf16)
+                mix[n, :, n4 * ranks * 4 : (n4 + 1) * ranks * 4] = table.T.astype(bf16)
         ret[me] = back[me]
 
         def came(e, _):
@@ -427,6 +464,14 @@
             small(k, 4).start()
         final[:, cols(t)] = moved[t]
         for k in range(1, 4):
+            small_arrived(k, 6).wait_recv()
+        for n in range(4):
+            at = slice(n * width, n * width + width)
+            out = jnp.zeros((32, width), f32)
+            for x in range(4):
+                out = out + jnp.dot(attx[x], wp[256 * x : 256 * x + 256, at], preferred_element_type=f32)
+            mixed_ref[:, at] = out.astype(bf16)
+        for k in range(1, 4):
             small_arrived(k, 4).wait_recv()
         o_ref[...] = final[...]
 
@@ -438,18 +483,25 @@
         drain(rows.at[0], send_sem.at[2])
         drain(hid.at[pl.ds(0, 2)], send_sem.at[3])
         drain(hid.at[0], send_sem.at[4])
-        drain(back.at[pl.ds(0, ranks - 1)], send_sem.at[21])
-        for kind in range(5):
+        drain(back.at[pl.ds(0, ranks - 1)], send_sem.at[27])
+        for kind in range(7):
             for k in range(1, 4):
                 small(k, kind).wait_send()
+        for d in range(2):
+            for step in range(1, 5):
+                along_z(d, step).wait_send()
+            for step in range(2):
+                along_y(d, step).wait_send()
+        for i in range(4):
+            across(i).wait_send()
 
     vmem = pl.BlockSpec(memory_space=pltpu.VMEM)
     hbm = pl.BlockSpec(memory_space=pl.ANY)
     return pl.pallas_call(
         kernel,
-        out_shape=jax.ShapeDtypeStruct(nx.shape, bf16),
-        in_specs=[vmem, vmem, vmem, hbm, hbm, hbm],
-        out_specs=vmem,
+        out_shape=(jax.ShapeDtypeStruct((32, nx.shape[1]), bf16), jax.ShapeDtypeStruct(nx.shape, bf16)),
+        in_specs=[vmem] * 5 + [hbm] * 6,
+        out_specs=(vmem, vmem),
         scratch_shapes=[
             pltpu.VMEM((4, 64, width), bf16),
             pltpu.VMEM((4, 8, 256), jnp.int32),
@@ -465,23 +517,35 @@
             pltpu.VMEM((4, 64, width), bf16),
             pltpu.VMEM(nx.shape, bf16),
             pltpu.VMEM((2, 256, ranks * 16), bf16),
-            pltpu.SemaphoreType.DMA((3,)),
+            pltpu.VMEM((4,) + latents.shape, bf16),
+            pltpu.VMEM(key_up.shape, bf16),
+            pltpu.VMEM(value_up.shape, bf16),
+            pltpu.VMEM(out_proj.shape, bf16),
+            pltpu.VMEM((8, depth, 544, 128), bf16),
+            pltpu.VMEM((2, 1, 256), f32),
+            pltpu.VMEM((2, 1, 256), f32),
+            pltpu.VMEM((2, 128, 256), f32),
+            pltpu.VMEM((4, 32, 256), bf16),
+            pltpu.VMEM((4, 32, 256), bf16),
+            pltpu.SemaphoreType.DMA((6,)),
             pltpu.SemaphoreType.DMA((1,)),
-            pltpu.SemaphoreType.DMA((5, 4)),
+            pltpu.SemaphoreType.DMA((7, 4)),
             pltpu.SemaphoreType.DMA((ranks,)),
             pltpu.SemaphoreType.DMA((ranks,)),
             pltpu.SemaphoreType.DMA((4, 2, 8)),
-            pltpu.SemaphoreType.DMA((22,)),
+            pltpu.SemaphoreType.DMA((28,)),
+            pltpu.SemaphoreType.DMA((16,)),
+            pltpu.SemaphoreType.DMA((16,)),
         ],
         compiler_params=pltpu.CompilerParams(
-            collective_id=0, has_side_effects=True, vmem_limit_bytes=40 << 20
+            collective_id=0, has_side_effects=True, vmem_limit_bytes=56 << 20
         ),
         cost_estimate=pl.CostEstimate(flops=5 * 10**9, bytes_accessed=3 * 10**7, transcendentals=0),
         name="exchange",
-    )(nx, where, share, w_gate, w_up, w_down)
-
-
-def expert_half(tokens, moe_gain, routes, group_prob, expert_prob, w_gate, w_up, w_down):
+    )(nx, where, share, latents, queries, w_gate, w_up, w_down, key_up, value_up, out_proj)
+
+
+def expert_inputs(tokens, moe_gain, routes, group_prob, expert_prob):
     row_count = tokens.shape[0]
     expert_count = lax.axis_size("ep")
     nx = rms_scale(tokens, moe_gain).astype(jnp.bfloat16)
@@ -495,7 +559,7 @@
     mine = (jnp.arange(256, dtype=jnp.int32) // 64 == t)[None, :]
     where = jnp.pad(jnp.where(mine, jnp.tile(target, (1, 4)), 0), ((0, 6), (0, 0)))
     share = jnp.pad(jnp.where(mine, jnp.tile(shares, (1, 4)), 0.0), ((0, 6), (0, 0)))
-    return exchange(nx, where, share, w_gate[0], w_up[0], w_down[0])
+    return nx, where, share
 
 
 def body(
@@ -515,9 +579,11 @@
     w_up,
     w_down,
 ):
-    mixed = mixer_half(query, latent, rope_key, latent_gain, key_up, value_up, out_proj)
-    moe_out = expert_half(tokens, moe_gain, routes, group_prob, expert_prob, w_gate, w_up, w_down)
-    return (mixed, moe_out)
+    nx, where, share = expert_inputs(tokens, moe_gain, routes, group_prob, expert_prob)
+    queries, latents = mixer_inputs(query, latent, rope_key, latent_gain)
+    return exchange(
+        nx, where, share, latents, queries, w_gate[0], w_up[0], w_down[0], key_up, value_up, out_proj
+    )
 
 
 def solution(mesh):

time: 245 us -> 137 us (0.56)
  waiting for transfers between devices: 85.7 us -> 0 us
  Pallas kernels: 111 us -> 126 us
  between operations: 14.4 us -> 0.96 us
  blocking collectives: 10.4 us -> 0 us
  matrix products: 5 us -> 0 us
  starting transfers between devices: 4.02 us -> 0 us
  local copies, waits for them, and re-layouts: 11.1 us -> 7.55 us
    all_gather x1 -> x0, waiting for transfers between devices: 85.7 us -> none  [mixer_half(): kv = lax.all_gather(kv, 'ep', axis=0)]
    pallas_call x2 -> x1, Pallas kernels: 111 us -> 126 us  [exchange(): pl.pallas_call(kernel, out_shape=(jax.ShapeDtypeStruct((32, nx.shape[1]),...]
    all_gather x1 -> x0, blocking collectives: 10.4 us -> none  [in_one_piece(): out, at, done = (lax.all_gather(both, axis, axis=dim, tiled=True), 0, [])]
    dot_general x3 -> x0, matrix products: 5 us -> none  [the longest x1 3.68 us: mixer_half(): jnp.dot(own_attention, out_proj, preferred_element_type=jnp.float32)]
    unnamed x24 -> x20, local copies, waits for them, and re-layouts: 8.67 us -> 4.38 us
    all_to_all x1 -> x0, starting transfers between devices: 3.98 us -> none  [mixer_half(): lax.all_to_all(attention, 'tp', split_axis=0, concat_axis=1, tiled=True)]
  transfers between devices with their start and end apart: 2 -> 0, of which waited for: 1 -> 0; matrix products, arithmetic and copies ran while one was open for 1% -> 0% of each run, Pallas kernels for 44% -> 0%
where the time goes in v3:
time: 137 us
  Pallas kernels  126 us (92%)
  local copies, waits for them, and re-layouts  7.55 us (6%)
  other arithmetic  2.95 us (2%)
    pallas_call x1, Pallas kernels, exchange(): pl.pallas_call(kernel, out_shape=(jax.ShapeDtypeStruct((32, nx.shape[1]),...  126 us
    unnamed x20, local copies, waits for them, and re-layouts  4.38 us

profile of v3, /device:TPU:1, one launch (start us, length us, event | category | flops | bytes accessed | tf_op | source)
XLA Modules:
  0.0 137.1 jit_solution(2325805245926400865)
XLA Ops:
  0.7 0.1 multiply_cosine_fusion.1
  0.9 1.0 copy.33
  2.3 1.3 copy.34
  3.6 0.1 fusion.79
  3.8 0.1 pad_maximum_fusion.1
  3.9 0.1 tile.32
  4.0 0.1 fusion.23
  4.1 0.1 fusion.25
  4.2 0.6 pad_maximum_fusion.lat_ref
  4.8 0.1 copy.31
  4.9 0.1 eq.37
  5.1 0.1 fusion.74
  5.2 0.2 reduce_window_sum.11
  5.3 0.2 select_reduce_fusion
  5.5 0.1 reduce_sum.40
  5.7 0.1 tile.13
  5.9 0.6 pad.86.where_ref
  6.5 0.1 tile.30
  6.6 0.6 pad.87.share_ref
  7.2 0.2 fusion
  7.4 0.8 fusion.2.nx_ref
  8.2 125.7 %exchange.1 = (bf16[32,2048]{1,0:T(8,128)(2,1)}, bf16[64,2048]{1,0:T(8,128)(2,1)}) custom-call(bf16[64,2048]{1,0:T(8,128)(2,1)} %fusion.2.nx_ref, s32[8,256]{1,0:T(8,128)} %pad.86.where_ref, f32[8,256]{1,0:T(8,128)} %pad.87.share_ref, bf16[32,640]{1,0:T(8,128)(2,1)} %pad_maximum_fusion.lat_ref, bf16[2,4,256,256]{3,2,1,0:T(8,128)(2,1)} %bitcast.93, ...), custom_call_target="tpu_custom_call" | custom-call | flops 5000000000 | bytes 30000000 | tf_op jit(solution)/shard_map/exchange/pallas_call | solution.py:500
  133.9 1.6 %copy.52 = bf16[32,2048]{1,0:T(8,128)(2,1)} copy(bf16[32,2048]{1,0:T(8,128)(2,1)} %get-tuple-element.18) | data formatting | bytes 262144
  135.4 1.7 %copy.53 = bf16[64,2048]{1,0:T(8,128)(2,1)} copy(bf16[64,2048]{1,0:T(8,128)(2,1)} %get-tuple-element.19) | data formatting | bytes 524288
  (56 shorter events, 0.5 us)
Async XLA Ops:
  0.6 3.0 %copy-start.3 = (bf16[32,32]{1,0:T(8,128)(2,1)S(1)}, bf16[32,32]{1,0:T(8,128)(2,1)}, u32[]{:S(2)}) copy-start(bf16[32,32]{1,0:T(8,128)(2,1)} %param.17) | copy-start | bytes 6148
  0.6 3.3 %copy-start.1 = (bf16[32,512]{1,0:T(8,128)(2,1)S(1)}, bf16[32,512]{1,0:T(8,128)(2,1)}, u32[]{:S(2)}) copy-start(bf16[32,512]{1,0:T(8,128)(2,1)} %param.16) | copy-start | bytes 98308
  0.7 3.5 %copy-start.6 = (f32[512]{0:T(512)S(1)}, f32[512]{0:T(512)}, u32[]{:S(2)}) copy-start(f32[512]{0:T(512)} %param.18) | copy-start | bytes 6148
  0.7 4.2 %copy-start.4 = (s32[64,2]{0,1:T(2,128)S(1)}, s32[64,2]{0,1:T(2,128)}, u32[]{:S(2)}) copy-start(s32[64,2]{0,1:T(2,128)} %param.24) | copy-start | bytes 1540
  0.7 5.8 %copy-start.5 = (f32[64,2]{0,1:T(2,128)S(1)}, f32[64,2]{0,1:T(2,128)}, u32[]{:S(2)}) copy-start(f32[64,2]{0,1:T(2,128)} %param.26) | copy-start | bytes 1540
  0.7 5.8 %copy-start.7 = (f32[64]{0:T(128)S(1)}, f32[64]{0:T(128)}, u32[]{:S(2)}) copy-start(f32[64]{0:T(128)} %param.25) | copy-start | bytes 772
  0.7 6.5 %copy-start = (bf16[64,2048]{1,0:T(8,128)(2,1)S(1)}, bf16[64,2048]{1,0:T(8,128)(2,1)}, u32[]{:S(2)}) copy-start(bf16[64,2048]{1,0:T(8,128)(2,1)} %param.22) | copy-start | bytes 786436
  0.7 6.7 %copy-start.2 = (f32[2048]{0:T(1024)S(1)}, f32[2048]{0:T(1024)}, u32[]{:S(2)}) copy-start(f32[2048]{0:T(1024)} %param.23) | copy-start | bytes 24580

commit v4 on v3

--- a/solution.py
+++ b/solution.py
@@ -11,66 +11,51 @@
 ROPE_DIM = 32
 MESH = pl.DeviceIdType.MESH
 
+ZW = (0, 1, 2, 3)
+SA = 5
+SB = 9
+SM = 1
+SF = 10
+LO = ((4, 1), (5, 2), (6, 3), (7, 4), (8, 5), (9, 6), (10, 7))
+HI = ((3, 1), (4, 2), (5, 3), (6, 4), (7, 5), (8, 6), (9, 7), (10, 8))
+
 
 epsilon = 1e-06
 rope_base = 10000.0
 masked_value = -1e30
 
 
-def rms_scale(values, gain):
-    widened = values.astype(jnp.float32)
-    return widened * lax.rsqrt(jnp.mean(widened * widened, axis=-1, keepdims=True) + epsilon) * gain
-
-
-def tables(positions, rope_width):
-    half_width = rope_width // 2
-    inverse = rope_base ** (-2.0 * jnp.arange(half_width, dtype=jnp.float32) / rope_width)
+def rotation(positions):
+    half_width = ROPE_DIM // 2
+    inverse = rope_base ** (-2.0 * jnp.arange(half_width, dtype=jnp.float32) / ROPE_DIM)
     angles = positions.astype(jnp.float32)[:, None] * inverse[None, :]
-    return (jnp.cos(angles), jnp.sin(angles))
-
-
-def rotate(values, cosine, sine):
-    half_width = values.shape[-1] // 2
-    lower = values[..., :half_width]
-    upper = values[..., half_width:]
-    return jnp.concatenate([lower * cosine - upper * sine, lower * sine + upper * cosine], axis=-1)
-
-
-def query_rows(query, positions):
-    rows = query.shape[0]
-    cosine, sine = tables(positions, ROPE_DIM)
-    heads = query.reshape(rows, 4, NOPE + ROPE_DIM)
-    turned = rotate(heads[..., NOPE:].astype(jnp.float32), cosine[:, None, :], sine[:, None, :])
-    turned = turned.astype(jnp.bfloat16).transpose(1, 0, 2)
-    flat = heads[..., :NOPE].transpose(1, 0, 2)
-    out = []
-    for p in range(2):
-        for j in range(4):
-            for i in range(2):
-                h = 2 * p + i
-                nope = jnp.pad(flat[h], ((0, 0), (64 * i, 64 - 64 * i)))
-                rope = jnp.pad(turned[h], ((0, 0), (32 * j, 96 - 32 * j)))
-                out.append(jnp.concatenate([nope, rope], axis=1))
-    return jnp.stack(out).reshape(2, 4, 256, 256)
-
-
-def mixer_inputs(query, latent, rope_key, latent_gain):
-    rows = query.shape[0]
-    own_rows = latent.shape[0]
-    t = lax.axis_index("tp")
-    query_start = lax.axis_index("ep") * rows
-    key_start = query_start + t * own_rows
-    normed = rms_scale(latent, latent_gain).astype(jnp.bfloat16)
-    key_cos, key_sin = tables(key_start + jnp.arange(own_rows, dtype=jnp.int32), ROPE_DIM)
-    rotated = rotate(rope_key.astype(jnp.float32), key_cos, key_sin)
-    mine = (jnp.arange(128, dtype=jnp.int32) // 32 == t)[None, :]
-    packed = jnp.where(mine, jnp.tile(rotated, (1, 4)), 0.0).astype(jnp.bfloat16)
-    queries = query_rows(query, query_start + jnp.arange(rows, dtype=jnp.int32))
-    return queries, jnp.concatenate([normed, packed], axis=1)
-
-
-def exchange(nx, where, share, latents, queries, w_gate, w_up, w_down, key_up, value_up, out_proj):
-    width = nx.shape[1] // 4
+    cosine, sine = jnp.cos(angles), jnp.sin(angles)
+    return jnp.concatenate([cosine, cosine, -sine, sine], axis=-1)
+
+
+def plain_copy(first, second):
+    def kernel(a_ref, b_ref, c_ref, d_ref):
+        c_ref[...] = a_ref[...]
+        d_ref[...] = b_ref[...]
+
+    vmem = pl.BlockSpec(memory_space=pltpu.VMEM)
+    return pl.pallas_call(
+        kernel,
+        out_shape=(
+            jax.ShapeDtypeStruct(first.shape, first.dtype),
+            jax.ShapeDtypeStruct(second.shape, second.dtype),
+        ),
+        in_specs=[vmem, vmem],
+        out_specs=(vmem, vmem),
+        name="plain_copy",
+    )(first, second)
+
+
+def exchange(
+    tokens, moe_gain, routes, group_prob, expert_prob, turn, latent, rope_key, latent_gain,
+    query, w_gate, w_up, w_down, key_up, value_up, out_proj,
+):
+    width = tokens.shape[1] // 4
     units = w_gate.shape[1]
     ranks = lax.axis_size("ep")
     depth = ranks // 8
@@ -78,10 +63,12 @@
     shift = math.log2(math.e) / math.sqrt(NOPE + ROPE_DIM)
 
     def kernel(
-        nx_ref, where_ref, share_ref, lat_ref, q_ref, wg_hbm, wu_hbm, wd_hbm, ku_hbm, vu_hbm, wp_hbm, mixed_ref, o_ref,
+        tok_hbm, gain_ref, routes_ref, group_ref, prob_ref, turn_ref, lat_hbm, rope_hbm, lgain_ref,
+        q_hbm, wg_hbm, wu_hbm, wd_hbm, ku_hbm, vu_hbm, wp_hbm, mixed_ref, o_ref,
+        tok, lin, rin, qin, nx_ref, where_ref, share_ref, lat_ref, q_ref, relay,
         xn, pos, shr, slab, rows, wg, wu, wd, hid, back, ret, moved, final, mix,
         lat, ku, vu, wp, kv, top, total, acc, attm, attx,
-        load_sem, own_sem, small_recv, arrive, ret_sem, ring_recv, send_sem, kv_recv, kv_send,
+        load_sem, own_sem, small_recv, arrive, ret_sem, ring_recv, send_sem, kv_recv, kv_send, relay_send, relay_recv,
     ):
         me, t = lax.axis_index("ep"), lax.axis_index("tp")
         z = me // 8
@@ -99,7 +86,13 @@
             pltpu.make_async_copy(ku_hbm, ku, load_sem.at[4]),
             pltpu.make_async_copy(vu_hbm, vu, load_sem.at[5]),
         ]
-        for load in early + loads:
+        first_loads = [
+            pltpu.make_async_copy(tok_hbm, tok, load_sem.at[6]),
+            pltpu.make_async_copy(lat_hbm, lin, load_sem.at[7]),
+            pltpu.make_async_copy(rope_hbm, rin, load_sem.at[8]),
+            pltpu.make_async_copy(q_hbm, qin, load_sem.at[9]),
+        ]
+        for load in first_loads + early + loads:
             load.start()
 
         barrier = pltpu.get_barrier_semaphore()
@@ -111,6 +104,42 @@
         lax.fori_loop(1, ranks, greet, 0)
         for k in range(1, 4):
             pl.semaphore_signal(barrier, inc=1, device_id=(me, lax.rem(t + k, 4)), device_id_type=MESH)
+
+        def normed(ref, gain):
+            wide = ref[...].astype(f32)
+            return wide * lax.rsqrt(jnp.mean(wide * wide, axis=-1, keepdims=True) + epsilon) * gain[...]
+
+        def turned(part, cosine, sine):
+            half = ROPE_DIM // 2
+            swapped = jnp.concatenate([part[:, half:], part[:, :half]], axis=1)
+            return part * cosine + swapped * sine
+
+        choice = routes_ref[...].astype(f32)
+        down_at = lax.broadcasted_iota(jnp.int32, (64, 64), 0)
+        across_at = lax.broadcasted_iota(jnp.int32, (64, 64), 1)
+        columns = [
+            jnp.sum(jnp.where(down_at == across_at, choice[k : k + 1], 0.0), axis=1, keepdims=True) for k in range(2)
+        ]
+        mine = lax.broadcasted_iota(jnp.int32, (1, 256), 1) // 64 == t
+        odds = prob_ref[...]
+        where_ref[...] = jnp.zeros(where_ref.shape, jnp.int32)
+        share_ref[...] = jnp.zeros(share_ref.shape, f32)
+        for k in range(2):
+            row = choice[k : k + 1]
+            same = jnp.where(columns[0] == row, 1.0, 0.0) + jnp.where(columns[1] == row, 1.0, 0.0)
+            slot = jnp.sum(jnp.where(down_at < across_at, same, 0.0), axis=0, keepdims=True)
+            target = (row * 16.0 + slot).astype(jnp.int32) + t * 4 + 1
+            portion = group_ref[...] * odds[k : k + 1] / (odds[0:1] + odds[1:2])
+            where_ref[k : k + 1] = jnp.where(mine, jnp.concatenate([target] * 4, axis=1), 0)
+            share_ref[k : k + 1] = jnp.where(mine, jnp.concatenate([portion] * 4, axis=1), 0.0)
+        for load in first_loads:
+            load.wait()
+        nx_ref[...] = normed(tok, gain_ref).astype(bf16)
+        lat_ref[:, : lin.shape[1]] = normed(lin, lgain_ref).astype(bf16)
+        table = turn_ref[pl.ds(pl.multiple_of(t * 32, 32), 32)]
+        own_key = turned(rin[...].astype(f32), table[:, :32], table[:, 32:])
+        own_lanes = lax.broadcasted_iota(jnp.int32, (32, 128), 1) // 32 == t
+        lat_ref[:, lin.shape[1] :] = jnp.where(own_lanes, jnp.concatenate([own_key] * 4, axis=1), 0.0).astype(bf16)
         pl.semaphore_wait(barrier, ranks + 2)
 
         def remote(s, d, send, recv, e, x):
@@ -144,9 +173,23 @@
             ref = (xn.at[x], pos.at[x], shr.at[x], wd.at[x], final.at[:, cols(x)], lat.at[x], attx.at[x])[kind]
             return remote(ref, ref, send_sem.at[5], recv, me, x)
 
-        for kind in (0, 1, 5, 2, 3):
+        def relayed(d, hop, arrived=False):
+            to = right if d == 0 else left
+            part = pl.ds(128 * d, 128)
+            if hop == 0:
+                source = relay.at[d] if arrived else wd_hbm.at[part, cols(lax.rem(t + 2, 4))]
+                return remote(source, relay.at[d], relay_send.at[d], relay_recv.at[d], me, to)
+            origin = lax.rem(t + 2, 4) if arrived else (left if d == 0 else right)
+            target = wd.at[origin, part]
+            return remote(target if arrived else relay.at[d], target, relay_send.at[2 + d], relay_recv.at[2 + d], me, to)
+
+        for kind in (0, 1, 5, 2):
             for k in (1, 3, 2):
                 small(k, kind).start()
+        for d in range(2):
+            relayed(d, 0).start()
+        for k in (1, 3):
+            small(k, 3).start()
         lat[t] = lat_ref[...]
         xn[t] = nx_ref[:, cols(t)]
         pos[t] = where_ref[...]
@@ -198,17 +241,20 @@
             n = 4 * d + step - 1
             return remote(ref, ref, kv_send.at[n], kv_recv.at[n], plane(sign) * 8 + g0, t)
 
-        def along_y(d, stage, arrived=False):
+        def along_y(d, block, arrived=False):
             sign = 1 if d == 0 else -1
-            hops = stage + (1 if arrived else 0)
-            col = column(-sign * hops)
-            ref = kv.at[col] if stage == 0 else kv.at[col, pl.ds(4 * d, 4)]
-            n = 8 + 2 * stage + d
+            ref = kv.at[column(-sign if arrived else 0), block]
+            n = 8 + 8 * d + block
             return remote(ref, ref, kv_send.at[n], kv_recv.at[n], z * 8 + column(sign), t)
+
+        def along_y2(d, arrived=False):
+            sign = 1 if d == 0 else -1
+            ref = kv.at[column(-sign * (2 if arrived else 1)), pl.ds(4 * d, 4)]
+            return remote(ref, ref, kv_send.at[24 + d], kv_recv.at[24 + d], z * 8 + column(sign), t)
 
         def across(i, arrived=False):
             ref = kv.at[column((0, -1, 1, 2)[i], 1 if arrived else 0)]
-            return remote(ref, ref, kv_send.at[12 + i], kv_recv.at[12 + i], z * 8 + column(0, 1), t)
+            return remote(ref, ref, kv_send.at[26 + i], kv_recv.at[26 + i], z * 8 + column(0, 1), t)
 
         dispatch(0, 0)
         for k in range(1, 4):
@@ -228,15 +274,23 @@
         kv[g0, z, 512:544] = packed.astype(bf16)
         for d in range(2):
             along_z(d, 1).start()
-        for step in range(1, 4):
-            lax.fori_loop(2 * step - 1, 2 * step + 1, dispatch, 0)
-            for d in range(2):
-                along_z(d, step, True).wait_recv()
-                along_z(d, step + 1).start()
-        dispatch(depth - 1, 0)
+            along_y(d, z).start()
+        lax.fori_loop(1, depth, dispatch, 0)
         own_slab().start()
+        for d in range(2):
+            relayed(d, 0, True).wait_recv()
+            relayed(d, 1).start()
         for k in range(1, 4):
             small_arrived(k, 2).wait_recv()
+        q_ref[...] = jnp.zeros(q_ref.shape, bf16)
+        asked = qin[...].astype(f32)
+        for h in range(4):
+            p, i = h // 2, h % 2
+            nope = asked[:, 96 * h : 96 * h + 64].astype(bf16)
+            rope = turned(asked[:, 96 * h + 64 : 96 * h + 96], turn_ref[:, :32], turn_ref[:, 32:]).astype(bf16)
+            for j in range(4):
+                q_ref[p, j, 128 * i : 128 * i + 128, 64 * i : 64 * i + 64] = nope
+                q_ref[p, j, 128 * i : 128 * i + 128, 128 + 32 * j : 160 + 32 * j] = rope
         top[...] = jnp.full(top.shape, masked_value, f32)
         total[...] = jnp.zeros(total.shape, f32)
         acc[...] = jnp.zeros(acc.shape, f32)
@@ -319,6 +373,16 @@
         def block_of(chunk):
             return lax.rem(z - offset(chunk) + depth, depth)
 
+        def mix_tables():
+            portion = shr[0] + shr[1] + shr[2] + shr[3]
+            high = portion.astype(bf16).astype(f32)
+            low = portion - high
+            for n4 in range(4):
+                row = lax.broadcasted_iota(jnp.int32, (ranks * 4, 256), 0) + n4 * ranks * 4
+                for n, part in enumerate((high, low)):
+                    table = jnp.where(row == first, part[0:1], 0.0) + jnp.where(row == second, part[1:2], 0.0)
+                    mix[n, :, n4 * ranks * 4 : (n4 + 1) * ranks * 4] = table.T.astype(bf16)
+
         def pick(s, table):
             out = jnp.int32(0)
             for at, value in table:
@@ -326,14 +390,6 @@
             return out
 
         def stage(s, _):
-            @pl.when(s == 1)
-            def _():
-                for d in range(2):
-                    along_z(d, 4, True).wait_recv()
-                for d in range(2):
-                    along_y(d, 0).start()
-                across(0).start()
-
             @pl.when(s < depth)
             def _():
                 block = block_of(s)
@@ -387,8 +443,10 @@
 
             @pl.when(s == 4)
             def _():
-                for k in range(1, 4):
+                for k in (1, 3):
                     small_arrived(k, 3).wait_recv()
+                for d in range(2):
+                    relayed(d, 1, True).wait_recv()
 
             @pl.when(s >= 4)
             def _():
@@ -412,24 +470,40 @@
 
                 lax.fori_loop(0, 8, send, 0)
 
-            @pl.when(s == 7)
-            def _():
-                for d in range(2):
-                    along_y(d, 0, True).wait_recv()
-                    along_y(d, 1).start()
+            for step in range(1, 5):
+
+                @pl.when(s == ZW[step - 1])
+                def _(step=step):
+                    for d in range(2):
+                        along_z(d, step, True).wait_recv()
+                        if step < 4:
+                            along_z(d, step + 1).start()
+                    for block in (plane(-step), plane(step)) if step < 4 else (plane(4),):
+                        for d in range(2):
+                            along_y(d, block).start()
+                    if step == 4:
+                        across(0).start()
+
+            @pl.when(s == SA)
+            def _():
+                for d in range(2):
+                    lax.fori_loop(0, depth, lambda b, _, d=d: (along_y(d, b, True).wait_recv(), 0)[1], 0)
+                    along_y2(d).start()
                     across(1 + d).start()
 
-            @pl.when(s == 10)
-            def _():
-                for d in range(2):
-                    along_y(d, 1, True).wait_recv()
+            @pl.when(s == SB)
+            def _():
+                for d in range(2):
+                    along_y2(d, True).wait_recv()
                 across(3).start()
 
-            lo = pick(s, ((3, 1), (8, 2), (9, 4), (10, 6), (11, 7)))
-            hi = pick(s, ((2, 1), (3, 2), (8, 4), (9, 6), (10, 7), (11, 8)))
-            lax.fori_loop(lo, hi, attend, 0)
-
-            @pl.when(s == 11)
+            @pl.when(s == SM)
+            def _():
+                mix_tables()
+
+            lax.fori_loop(pick(s, LO), pick(s, HI), attend, 0)
+
+            @pl.when(s == SF)
             def _():
                 attended()
 
@@ -437,14 +511,6 @@
 
         lax.fori_loop(0, depth + 4, stage, 0)
 
-        portion = shr[0] + shr[1] + shr[2] + shr[3]
-        high = portion.astype(bf16).astype(f32)
-        low = portion - high
-        for n4 in range(4):
-            row = lax.broadcasted_iota(jnp.int32, (ranks * 4, 256), 0) + n4 * ranks * 4
-            for n, part in enumerate((high, low)):
-                table = jnp.where(row == first, part[0:1], 0.0) + jnp.where(row == second, part[1:2], 0.0)
-                mix[n, :, n4 * ranks * 4 : (n4 + 1) * ranks * 4] = table.T.astype(bf16)
         ret[me] = back[me]
 
         def came(e, _):
@@ -486,12 +552,16 @@
         drain(back.at[pl.ds(0, ranks - 1)], send_sem.at[27])
         for kind in range(7):
             for k in range(1, 4):
-                small(k, kind).wait_send()
+                if (k, kind) != (2, 3):
+                    small(k, kind).wait_send()
+        for d in range(2):
+            for hop in range(2):
+                relayed(d, hop).wait_send()
         for d in range(2):
             for step in range(1, 5):
                 along_z(d, step).wait_send()
-            for step in range(2):
-                along_y(d, step).wait_send()
+            lax.fori_loop(0, depth, lambda b, _, d=d: (along_y(d, b).wait_send(), 0)[1], 0)
+            along_y2(d).wait_send()
         for i in range(4):
             across(i).wait_send()
 
@@ -499,10 +569,20 @@
     hbm = pl.BlockSpec(memory_space=pl.ANY)
     return pl.pallas_call(
         kernel,
-        out_shape=(jax.ShapeDtypeStruct((32, nx.shape[1]), bf16), jax.ShapeDtypeStruct(nx.shape, bf16)),
-        in_specs=[vmem] * 5 + [hbm] * 6,
+        out_shape=(jax.ShapeDtypeStruct((32, tokens.shape[1]), bf16), jax.ShapeDtypeStruct(tokens.shape, bf16)),
+        in_specs=[hbm] + [vmem] * 5 + [hbm] * 2 + [vmem] + [hbm] * 7,
         out_specs=(vmem, vmem),
         scratch_shapes=[
+            pltpu.VMEM(tokens.shape, bf16),
+            pltpu.VMEM(latent.shape, bf16),
+            pltpu.VMEM(rope_key.shape, bf16),
+            pltpu.VMEM(query.shape, bf16),
+            pltpu.VMEM(tokens.shape, bf16),
+            pltpu.VMEM((8, 256), jnp.int32),
+            pltpu.VMEM((8, 256), f32),
+            pltpu.VMEM((32, latent.shape[1] + 128), bf16),
+            pltpu.VMEM((2, 4, 256, 256), bf16),
+            pltpu.VMEM((2, 128, width), bf16),
             pltpu.VMEM((4, 64, width), bf16),
             pltpu.VMEM((4, 8, 256), jnp.int32),
             pltpu.VMEM((4, 8, 256), f32),
@@ -515,9 +595,9 @@
             pltpu.VMEM((ranks, 16, width), bf16),
             pltpu.VMEM((ranks, 16, width), bf16),
             pltpu.VMEM((4, 64, width), bf16),
-            pltpu.VMEM(nx.shape, bf16),
+            pltpu.VMEM(tokens.shape, bf16),
             pltpu.VMEM((2, 256, ranks * 16), bf16),
-            pltpu.VMEM((4,) + latents.shape, bf16),
+            pltpu.VMEM((4, 32, latent.shape[1] + 128), bf16),
             pltpu.VMEM(key_up.shape, bf16),
             pltpu.VMEM(value_up.shape, bf16),
             pltpu.VMEM(out_proj.shape, bf16),
@@ -527,39 +607,27 @@
             pltpu.VMEM((2, 128, 256), f32),
             pltpu.VMEM((4, 32, 256), bf16),
             pltpu.VMEM((4, 32, 256), bf16),
-            pltpu.SemaphoreType.DMA((6,)),
+            pltpu.SemaphoreType.DMA((10,)),
             pltpu.SemaphoreType.DMA((1,)),
             pltpu.SemaphoreType.DMA((7, 4)),
             pltpu.SemaphoreType.DMA((ranks,)),
             pltpu.SemaphoreType.DMA((ranks,)),
             pltpu.SemaphoreType.DMA((4, 2, 8)),
             pltpu.SemaphoreType.DMA((28,)),
-            pltpu.SemaphoreType.DMA((16,)),
-            pltpu.SemaphoreType.DMA((16,)),
+            pltpu.SemaphoreType.DMA((30,)),
+            pltpu.SemaphoreType.DMA((30,)),
+            pltpu.SemaphoreType.DMA((4,)),
+            pltpu.SemaphoreType.DMA((4,)),
         ],
         compiler_params=pltpu.CompilerParams(
             collective_id=0, has_side_effects=True, vmem_limit_bytes=56 << 20
         ),
         cost_estimate=pl.CostEstimate(flops=5 * 10**9, bytes_accessed=3 * 10**7, transcendentals=0),
         name="exchange",
-    )(nx, where, share, latents, queries, w_gate, w_up, w_down, key_up, value_up, out_proj)
-
-
-def expert_inputs(tokens, moe_gain, routes, group_prob, expert_prob):
-    row_count = tokens.shape[0]
-    expert_count = lax.axis_size("ep")
-    nx = rms_scale(tokens, moe_gain).astype(jnp.bfloat16)
-    flat = routes.reshape(-1)
-    onehot = (flat[:, None] == jnp.arange(expert_count, dtype=jnp.int32)[None, :]).astype(jnp.int32)
-    earlier = jnp.cumsum(onehot, axis=0) - onehot
-    slot = jnp.sum(earlier * onehot, axis=1)
-    t = lax.axis_index("tp")
-    target = (flat * 16 + t * 4 + slot + 1).reshape(row_count, 2).T
-    shares = (group_prob[:, None] * expert_prob / jnp.sum(expert_prob, axis=1, keepdims=True)).T
-    mine = (jnp.arange(256, dtype=jnp.int32) // 64 == t)[None, :]
-    where = jnp.pad(jnp.where(mine, jnp.tile(target, (1, 4)), 0), ((0, 6), (0, 0)))
-    share = jnp.pad(jnp.where(mine, jnp.tile(shares, (1, 4)), 0.0), ((0, 6), (0, 0)))
-    return nx, where, share
+    )(
+        tokens, moe_gain, routes, group_prob, expert_prob, turn, latent, rope_key, latent_gain,
+        query, w_gate, w_up, w_down, key_up, value_up, out_proj,
+    )
 
 
 def body(
@@ -579,11 +647,13 @@
     w_up,
     w_down,
 ):
-    nx, where, share = expert_inputs(tokens, moe_gain, routes, group_prob, expert_prob)
-    queries, latents = mixer_inputs(query, latent, rope_key, latent_gain)
-    return exchange(
-        nx, where, share, latents, queries, w_gate[0], w_up[0], w_down[0], key_up, value_up, out_proj
+    rows = query.shape[0]
+    turn = rotation(lax.axis_index("ep") * rows + jnp.arange(rows, dtype=jnp.int32))
+    mixed, moe_out = exchange(
+        tokens, moe_gain[None], routes.T, group_prob[None], expert_prob.T, turn, latent, rope_key, latent_gain[None],
+        query, w_gate[0], w_up[0], w_down[0], key_up, value_up, out_proj,
     )
+    return plain_copy(mixed, moe_out)
 
 
 def solution(mesh):

time: 137 us -> 117 us (0.85)
  Pallas kernels: 126 us -> 115 us
  local copies, waits for them, and re-layouts: 7.55 us -> 0 us
  other arithmetic: 2.95 us -> 1.08 us
    pallas_call x1 -> x2, Pallas kernels: 126 us -> 115 us  [the longest x1 113 us: exchange(): pl.pallas_call(kernel, out_shape=(jax.ShapeDtypeStruct((32, tokens.shape[...]
    unnamed x20 -> x0, local copies, waits for them, and re-layouts: 4.38 us -> none
    another operation x7 -> x0, local copies, waits for them, and re-layouts: 1.61 us -> none  [the longest x1 1.33 us: query_rows(): return jnp.stack(out).reshape(2, 4, 256, 256)]
where the time goes in v4:
time: 117 us
  Pallas kernels  115 us (98%)
    pallas_call x1, Pallas kernels, exchange(): pl.pallas_call(kernel, out_shape=(jax.ShapeDtypeStruct((32, tokens.shape[...  113 us

profile of v4, /device:TPU:1, one launch (start us, length us, event | category | flops | bytes accessed | tf_op | source)
XLA Modules:
  0.0 117.0 jit_solution(17121690213115923965)
XLA Ops:
  0.7 0.3 multiply_cosine_fusion
  1.0 0.8 pad_maximum_fusion.turn_ref
  1.7 113.5 %exchange.1 = (bf16[32,2048]{1,0:T(8,128)(2,1)}, bf16[64,2048]{1,0:T(8,128)(2,1)}) custom-call(bf16[64,2048]{1,0:T(8,128)(2,1)} %tok_hbm.1, f32[1,2048]{1,0:T(1,128)} %bitcast.11, s32[2,64]{1,0:T(2,128)} %bitcast.13, f32[1,64]{1,0:T(1,128)} %bitcast.15, f32[2,64]{1,0:T(2,128)} %bitcast.14, f32[128,64]{1,0:T(8,128)} %pad_maximum_fusion.turn_ref, ...), custom_call_target="tpu_custom_call" | custom-call | flops 5000000000 | bytes 30000000 | tf_op jit(solution)/shard_map/exchange/pallas_call | solution.py:570
  115.2 1.8 %plain_copy.1 = (bf16[32,2048]{1,0:T(8,128)(2,1)}, bf16[64,2048]{1,0:T(8,128)(2,1)}) custom-call(bf16[32,2048]{1,0:T(8,128)(2,1)} %get-tuple-element.4.a_ref, bf16[64,2048]{1,0:T(8,128)(2,1)} %get-tuple-element.5.b_ref), custom_call_target="tpu_custom_call" | custom-call | tf_op jit(solution)/shard_map/plain_copy/pallas_call | solution.py:42
  (2 shorter events, 0.0 us)

commit v5 on v4

--- a/solution.py
+++ b/solution.py
@@ -2,6 +2,7 @@
 
 import jax
 import jax.numpy as jnp
+import numpy as np
 from jax import lax
 from jax.experimental import pallas as pl
 from jax.experimental.pallas import tpu as pltpu
@@ -11,13 +12,13 @@
 ROPE_DIM = 32
 MESH = pl.DeviceIdType.MESH
 
-ZW = (0, 1, 2, 3)
-SA = 5
+ZW = (1, 2, 3, 4)
+SA = 6
 SB = 9
 SM = 1
-SF = 10
-LO = ((4, 1), (5, 2), (6, 3), (7, 4), (8, 5), (9, 6), (10, 7))
-HI = ((3, 1), (4, 2), (5, 3), (6, 4), (7, 5), (8, 6), (9, 7), (10, 8))
+SF = 11
+LO = ((5, 0), (7, 2), (8, 4), (10, 6), (11, 7))
+HI = ((5, 2), (7, 4), (8, 6), (10, 7), (11, 8))
 
 
 epsilon = 1e-06
@@ -26,11 +27,9 @@
 
 
 def rotation(positions):
-    half_width = ROPE_DIM // 2
-    inverse = rope_base ** (-2.0 * jnp.arange(half_width, dtype=jnp.float32) / ROPE_DIM)
-    angles = positions.astype(jnp.float32)[:, None] * inverse[None, :]
-    cosine, sine = jnp.cos(angles), jnp.sin(angles)
-    return jnp.concatenate([cosine, cosine, -sine, sine], axis=-1)
+    inverse = rope_base ** (-2.0 * np.arange(ROPE_DIM // 2) / ROPE_DIM)
+    angles = np.tile(positions[:, None] * inverse[None, :], (1, 2))
+    return jnp.asarray(np.concatenate([np.cos(angles), np.sin(angles)], axis=1), jnp.float32)
 
 
 def plain_copy(first, second):
@@ -52,7 +51,7 @@
 
 
 def exchange(
-    tokens, moe_gain, routes, group_prob, expert_prob, turn, latent, rope_key, latent_gain,
+    tokens, moe_gain, routes, group_prob, expert_prob, within, starts, latent, rope_key, latent_gain,
     query, w_gate, w_up, w_down, key_up, value_up, out_proj,
 ):
     width = tokens.shape[1] // 4
@@ -63,12 +62,12 @@
     shift = math.log2(math.e) / math.sqrt(NOPE + ROPE_DIM)
 
     def kernel(
-        tok_hbm, gain_ref, routes_ref, group_ref, prob_ref, turn_ref, lat_hbm, rope_hbm, lgain_ref,
+        tok_hbm, gain_ref, routes_ref, group_ref, prob_ref, within_ref, starts_ref, lat_hbm, rope_hbm, lgain_ref,
         q_hbm, wg_hbm, wu_hbm, wd_hbm, ku_hbm, vu_hbm, wp_hbm, mixed_ref, o_ref,
-        tok, lin, rin, qin, nx_ref, where_ref, share_ref, lat_ref, q_ref, relay,
-        xn, pos, shr, slab, rows, wg, wu, wd, hid, back, ret, moved, final, mix,
+        tok, lin, rin, qin, nx_ref, note_ref, lat_ref, q_ref, turn_ref,
+        xn, note, slab, rows, wg, wu, wd, hid, back, ret, moved, final, mix,
         lat, ku, vu, wp, kv, top, total, acc, attm, attx,
-        load_sem, own_sem, small_recv, arrive, ret_sem, ring_recv, send_sem, kv_recv, kv_send, relay_send, relay_recv,
+        load_sem, own_sem, small_recv, arrive, ret_sem, ring_recv, send_sem, kv_recv, kv_send,
     ):
         me, t = lax.axis_index("ep"), lax.axis_index("tp")
         z = me // 8
@@ -120,22 +119,24 @@
         columns = [
             jnp.sum(jnp.where(down_at == across_at, choice[k : k + 1], 0.0), axis=1, keepdims=True) for k in range(2)
         ]
-        mine = lax.broadcasted_iota(jnp.int32, (1, 256), 1) // 64 == t
         odds = prob_ref[...]
-        where_ref[...] = jnp.zeros(where_ref.shape, jnp.int32)
-        share_ref[...] = jnp.zeros(share_ref.shape, f32)
+        note_ref[...] = jnp.zeros(note_ref.shape, f32)
         for k in range(2):
             row = choice[k : k + 1]
             same = jnp.where(columns[0] == row, 1.0, 0.0) + jnp.where(columns[1] == row, 1.0, 0.0)
             slot = jnp.sum(jnp.where(down_at < across_at, same, 0.0), axis=0, keepdims=True)
-            target = (row * 16.0 + slot).astype(jnp.int32) + t * 4 + 1
-            portion = group_ref[...] * odds[k : k + 1] / (odds[0:1] + odds[1:2])
-            where_ref[k : k + 1] = jnp.where(mine, jnp.concatenate([target] * 4, axis=1), 0)
-            share_ref[k : k + 1] = jnp.where(mine, jnp.concatenate([portion] * 4, axis=1), 0.0)
+            note_ref[k : k + 1, 0:64] = row * 16.0 + slot + (t * 4).astype(f32)
+            note_ref[2 + k : 3 + k, 0:64] = group_ref[...] * odds[k : k + 1] / (odds[0:1] + odds[1:2])
         for load in first_loads:
             load.wait()
         nx_ref[...] = normed(tok, gain_ref).astype(bf16)
         lat_ref[:, : lin.shape[1]] = normed(lin, lgain_ref).astype(bf16)
+        near, far = within_ref[...], starts_ref[pl.ds(me, 1)]
+        near_cos, near_sin, far_cos, far_sin = near[:, :32], near[:, 32:], far[:, :32], far[:, 32:]
+        sine = near_sin * far_cos + near_cos * far_sin
+        lower = lax.broadcasted_iota(jnp.int32, sine.shape, 1) < ROPE_DIM // 2
+        turn_ref[:, :32] = near_cos * far_cos - near_sin * far_sin
+        turn_ref[:, 32:] = jnp.where(lower, -sine, sine)
         table = turn_ref[pl.ds(pl.multiple_of(t * 32, 32), 32)]
         own_key = turned(rin[...].astype(f32), table[:, :32], table[:, 32:])
         own_lanes = lax.broadcasted_iota(jnp.int32, (32, 128), 1) // 32 == t
@@ -156,9 +157,7 @@
             if kind == 0:
                 return remote(nx_ref.at[:, cols(x)], xn.at[t], send, recv, me, x)
             if kind == 1:
-                return remote(where_ref, pos.at[t], send, recv, me, x)
-            if kind == 2:
-                return remote(share_ref, shr.at[t], send, recv, me, x)
+                return remote(note_ref, note.at[t], send, recv, me, x)
             if kind == 3:
                 return remote(wd_hbm.at[:, cols(x)], wd.at[t], send, recv, me, x)
             if kind == 4:
@@ -170,41 +169,25 @@
         def small_arrived(k, kind):
             x = lax.rem(t + k, 4)
             recv = small_recv.at[kind, x]
-            ref = (xn.at[x], pos.at[x], shr.at[x], wd.at[x], final.at[:, cols(x)], lat.at[x], attx.at[x])[kind]
+            ref = (xn.at[x], note.at[x], None, wd.at[x], final.at[:, cols(x)], lat.at[x], attx.at[x])[kind]
             return remote(ref, ref, send_sem.at[5], recv, me, x)
 
-        def relayed(d, hop, arrived=False):
-            to = right if d == 0 else left
-            part = pl.ds(128 * d, 128)
-            if hop == 0:
-                source = relay.at[d] if arrived else wd_hbm.at[part, cols(lax.rem(t + 2, 4))]
-                return remote(source, relay.at[d], relay_send.at[d], relay_recv.at[d], me, to)
-            origin = lax.rem(t + 2, 4) if arrived else (left if d == 0 else right)
-            target = wd.at[origin, part]
-            return remote(target if arrived else relay.at[d], target, relay_send.at[2 + d], relay_recv.at[2 + d], me, to)
-
-        for kind in (0, 1, 5, 2):
-            for k in (1, 3, 2):
+        for kind in (0, 1, 5, 3):
+            for k in (2, 1, 3):
                 small(k, kind).start()
-        for d in range(2):
-            relayed(d, 0).start()
-        for k in (1, 3):
-            small(k, 3).start()
         lat[t] = lat_ref[...]
         xn[t] = nx_ref[:, cols(t)]
-        pos[t] = where_ref[...]
-        shr[t] = share_ref[...]
+        note[t] = note_ref[...]
         for kind in range(2):
             for k in range(1, 4):
                 small_arrived(k, kind).wait_recv()
 
-        place = pos[0] + pos[1] + pos[2] + pos[3] - 1
-        first, second = place[0:1], place[1:2]
+        notes = jnp.concatenate([note[x, :, 0:64] for x in range(4)], axis=1)
+        first, second = notes[0:1].astype(jnp.int32), notes[1:2].astype(jnp.int32)
         tokens = xn[...].reshape(256, width)
 
         def offset(i):
-            half = (i + 1) // 2
-            return jnp.where(lax.rem(i, 2) == 1, depth // 2 - half, depth // 2 + half)
+            return jnp.where(i == 6, 7, jnp.where(i == 5, 1, jnp.where(i == 4, 5, jnp.where(i == 3, 3, jnp.where(i == 2, 4, jnp.where(i == 1, 6, jnp.where(i == 0, 2, jnp.int32(0))))))))
 
         def own_slab():
             return pltpu.make_async_copy(slab.at[me], rows.at[t, me], own_sem.at[0])
@@ -277,11 +260,6 @@
             along_y(d, z).start()
         lax.fori_loop(1, depth, dispatch, 0)
         own_slab().start()
-        for d in range(2):
-            relayed(d, 0, True).wait_recv()
-            relayed(d, 1).start()
-        for k in range(1, 4):
-            small_arrived(k, 2).wait_recv()
         q_ref[...] = jnp.zeros(q_ref.shape, bf16)
         asked = qin[...].astype(f32)
         for h in range(4):
@@ -374,14 +352,10 @@
             return lax.rem(z - offset(chunk) + depth, depth)
 
         def mix_tables():
-            portion = shr[0] + shr[1] + shr[2] + shr[3]
-            high = portion.astype(bf16).astype(f32)
-            low = portion - high
             for n4 in range(4):
                 row = lax.broadcasted_iota(jnp.int32, (ranks * 4, 256), 0) + n4 * ranks * 4
-                for n, part in enumerate((high, low)):
-                    table = jnp.where(row == first, part[0:1], 0.0) + jnp.where(row == second, part[1:2], 0.0)
-                    mix[n, :, n4 * ranks * 4 : (n4 + 1) * ranks * 4] = table.T.astype(bf16)
+                table = jnp.where(row == first, notes[2:3], 0.0) + jnp.where(row == second, notes[3:4], 0.0)
+                mix[:, n4 * ranks * 4 : (n4 + 1) * ranks * 4] = table.T.astype(bf16)
 
         def pick(s, table):
             out = jnp.int32(0)
@@ -443,10 +417,8 @@
 
             @pl.when(s == 4)
             def _():
-                for k in (1, 3):
+                for k in range(1, 4):
                     small_arrived(k, 3).wait_recv()
-                for d in range(2):
-                    relayed(d, 1, True).wait_recv()
 
             @pl.when(s >= 4)
             def _():
@@ -522,9 +494,7 @@
 
         lax.fori_loop(0, ranks, came, 0)
         given = ret[...].reshape(ranks * 16, width)
-        summed = jnp.dot(mix[0], given, preferred_element_type=f32) + jnp.dot(
-            mix[1], given, preferred_element_type=f32
-        )
+        summed = jnp.dot(mix[...], given, preferred_element_type=f32)
         moved[...] = summed.astype(bf16).reshape(4, 64, width)
         for k in (1, 3, 2):
             small(k, 4).start()
@@ -550,13 +520,9 @@
         drain(hid.at[pl.ds(0, 2)], send_sem.at[3])
         drain(hid.at[0], send_sem.at[4])
         drain(back.at[pl.ds(0, ranks - 1)], send_sem.at[27])
-        for kind in range(7):
+        for kind in (0, 1, 3, 4, 5, 6):
             for k in range(1, 4):
-                if (k, kind) != (2, 3):
-                    small(k, kind).wait_send()
-        for d in range(2):
-            for hop in range(2):
-                relayed(d, hop).wait_send()
+                small(k, kind).wait_send()
         for d in range(2):
             for step in range(1, 5):
                 along_z(d, step).wait_send()
@@ -570,7 +536,7 @@
     return pl.pallas_call(
         kernel,
         out_shape=(jax.ShapeDtypeStruct((32, tokens.shape[1]), bf16), jax.ShapeDtypeStruct(tokens.shape, bf16)),
-        in_specs=[hbm] + [vmem] * 5 + [hbm] * 2 + [vmem] + [hbm] * 7,
+        in_specs=[hbm] + [vmem] * 6 + [hbm] * 2 + [vmem] + [hbm] * 7,
         out_specs=(vmem, vmem),
         scratch_shapes=[
             pltpu.VMEM(tokens.shape, bf16),
@@ -578,14 +544,12 @@
             pltpu.VMEM(rope_key.shape, bf16),
             pltpu.VMEM(query.shape, bf16),
             pltpu.VMEM(tokens.shape, bf16),
-            pltpu.VMEM((8, 256), jnp.int32),
-            pltpu.VMEM((8, 256), f32),
+            pltpu.VMEM((8, 128), f32),
             pltpu.VMEM((32, latent.shape[1] + 128), bf16),
             pltpu.VMEM((2, 4, 256, 256), bf16),
-            pltpu.VMEM((2, 128, width), bf16),
+            pltpu.VMEM((128, 64), f32),
             pltpu.VMEM((4, 64, width), bf16),
-            pltpu.VMEM((4, 8, 256), jnp.int32),
-            pltpu.VMEM((4, 8, 256), f32),
+            pltpu.VMEM((4, 8, 128), f32),
             pltpu.VMEM((ranks, 16, width), bf16),
             pltpu.VMEM((4, ranks, 16, width), bf16),
             pltpu.VMEM(w_gate.shape, bf16),
@@ -596,7 +560,7 @@
             pltpu.VMEM((ranks, 16, width), bf16),
             pltpu.VMEM((4, 64, width), bf16),
             pltpu.VMEM(tokens.shape, bf16),
-            pltpu.VMEM((2, 256, ranks * 16), bf16),
+            pltpu.VMEM((256, ranks * 16), bf16),
             pltpu.VMEM((4, 32, latent.shape[1] + 128), bf16),
             pltpu.VMEM(key_up.shape, bf16),
             pltpu.VMEM(value_up.shape, bf16),
@@ -616,8 +580,6 @@
             pltpu.SemaphoreType.DMA((28,)),
             pltpu.SemaphoreType.DMA((30,)),
             pltpu.SemaphoreType.DMA((30,)),
-            pltpu.SemaphoreType.DMA((4,)),
-            pltpu.SemaphoreType.DMA((4,)),
         ],
         compiler_params=pltpu.CompilerParams(
             collective_id=0, has_side_effects=True, vmem_limit_bytes=56 << 20
@@ -625,7 +587,7 @@
         cost_estimate=pl.CostEstimate(flops=5 * 10**9, bytes_accessed=3 * 10**7, transcendentals=0),
         name="exchange",
     )(
-        tokens, moe_gain, routes, group_prob, expert_prob, turn, latent, rope_key, latent_gain,
+        tokens, moe_gain, routes, group_prob, expert_prob, within, starts, latent, rope_key, latent_gain,
         query, w_gate, w_up, w_down, key_up, value_up, out_proj,
     )
 
@@ -648,9 +610,9 @@
     w_down,
 ):
     rows = query.shape[0]
-    turn = rotation(lax.axis_index("ep") * rows + jnp.arange(rows, dtype=jnp.int32))
+    within, starts = rotation(np.arange(rows)), rotation(np.arange(lax.axis_size("ep")) * rows)
     mixed, moe_out = exchange(
-        tokens, moe_gain[None], routes.T, group_prob[None], expert_prob.T, turn, latent, rope_key, latent_gain[None],
+        tokens, moe_gain[None], routes.T, group_prob[None], expert_prob.T, within, starts, latent, rope_key, latent_gain[None],
         query, w_gate[0], w_up[0], w_down[0], key_up, value_up, out_proj,
     )
     return plain_copy(mixed, moe_out)

time: 117 us -> 113 us (0.966)
  Pallas kernels: 115 us -> 112 us
    pallas_call x1, Pallas kernels: 113 us -> 111 us  [exchange(): pl.pallas_call(kernel, out_shape=(jax.ShapeDtypeStruct((32, tokens.shape[...]
where the time goes in v5:
time: 113 us
  Pallas kernels  112 us (99%)
    pallas_call x1, Pallas kernels, exchange(): pl.pallas_call(kernel, out_shape=(jax.ShapeDtypeStruct((32, tokens.shape[...  111 us

profile of v5, /device:TPU:1, one launch (start us, length us, event | category | flops | bytes accessed | tf_op | source)
XLA Modules:
  0.0 113.0 jit_solution(9131450834614199385)
XLA Ops:
  0.6 110.6 %exchange.1 = (bf16[32,2048]{1,0:T(8,128)(2,1)}, bf16[64,2048]{1,0:T(8,128)(2,1)}) custom-call(bf16[64,2048]{1,0:T(8,128)(2,1)} %tok_hbm.1, f32[1,2048]{1,0:T(1,128)} %bitcast.11, s32[2,64]{1,0:T(2,128)} %bitcast.13, f32[1,64]{1,0:T(1,128)} %bitcast.15, f32[2,64]{1,0:T(2,128)} %bitcast.14, f32[128,64]{1,0:T(8,128)} %constant.4.clone.within_ref, ...), custom_call_target="tpu_custom_call" | custom-call | flops 5000000000 | bytes 30000000 | tf_op jit(solution)/shard_map/exchange/pallas_call | solution.py:536
  111.2 1.8 %plain_copy.1 = (bf16[32,2048]{1,0:T(8,128)(2,1)}, bf16[64,2048]{1,0:T(8,128)(2,1)}) custom-call(bf16[32,2048]{1,0:T(8,128)(2,1)} %get-tuple-element.4.a_ref, bf16[64,2048]{1,0:T(8,128)(2,1)} %get-tuple-element.5.b_ref), custom_call_target="tpu_custom_call" | custom-call | tf_op jit(solution)/shard_map/plain_copy/pallas_call | solution.py:41

commit v6 on v5

--- a/solution.py
+++ b/solution.py
@@ -62,9 +62,9 @@
     shift = math.log2(math.e) / math.sqrt(NOPE + ROPE_DIM)
 
     def kernel(
-        tok_hbm, gain_ref, routes_ref, group_ref, prob_ref, within_ref, starts_ref, lat_hbm, rope_hbm, lgain_ref,
+        tok_hbm, gain_hbm, routes_hbm, group_hbm, prob_hbm, within_hbm, starts_hbm, lat_hbm, rope_hbm, lgain_hbm,
         q_hbm, wg_hbm, wu_hbm, wd_hbm, ku_hbm, vu_hbm, wp_hbm, mixed_ref, o_ref,
-        tok, lin, rin, qin, nx_ref, note_ref, lat_ref, q_ref, turn_ref,
+        gain_ref, routes_ref, group_ref, prob_ref, within_ref, starts_ref, lgain_ref, tok, lin, rin, qin, nx_ref, note_ref, lat_ref, q_ref, turn_ref,
         xn, note, slab, rows, wg, wu, wd, hid, back, ret, moved, final, mix,
         lat, ku, vu, wp, kv, top, total, acc, attm, attx,
         load_sem, own_sem, small_recv, arrive, ret_sem, ring_recv, send_sem, kv_recv, kv_send,
@@ -85,13 +85,22 @@
             pltpu.make_async_copy(ku_hbm, ku, load_sem.at[4]),
             pltpu.make_async_copy(vu_hbm, vu, load_sem.at[5]),
         ]
+        small_loads = [
+            pltpu.make_async_copy(gain_hbm, gain_ref, load_sem.at[10]),
+            pltpu.make_async_copy(routes_hbm, routes_ref, load_sem.at[11]),
+            pltpu.make_async_copy(group_hbm, group_ref, load_sem.at[12]),
+            pltpu.make_async_copy(prob_hbm, prob_ref, load_sem.at[13]),
+            pltpu.make_async_copy(within_hbm, within_ref, load_sem.at[14]),
+            pltpu.make_async_copy(starts_hbm, starts_ref, load_sem.at[15]),
+            pltpu.make_async_copy(lgain_hbm, lgain_ref, load_sem.at[16]),
+        ]
         first_loads = [
             pltpu.make_async_copy(tok_hbm, tok, load_sem.at[6]),
             pltpu.make_async_copy(lat_hbm, lin, load_sem.at[7]),
             pltpu.make_async_copy(rope_hbm, rin, load_sem.at[8]),
             pltpu.make_async_copy(q_hbm, qin, load_sem.at[9]),
         ]
-        for load in first_loads + early + loads:
+        for load in small_loads + first_loads + early + loads:
             load.start()
 
         barrier = pltpu.get_barrier_semaphore()
@@ -100,7 +109,12 @@
             pl.semaphore_signal(barrier, inc=1, device_id=(lax.rem(me + k, ranks), t), device_id_type=MESH)
             return 0
 
-        lax.fori_loop(1, ranks, greet, 0)
+        def greet_both(k, _):
+            greet(ranks // 2 + k, 0)
+            return greet(ranks // 2 - k, 0)
+
+        greet(ranks // 2, 0)
+        lax.fori_loop(1, ranks // 2, greet_both, 0)
         for k in range(1, 4):
             pl.semaphore_signal(barrier, inc=1, device_id=(me, lax.rem(t + k, 4)), device_id_type=MESH)
 
@@ -113,6 +127,8 @@
             swapped = jnp.concatenate([part[:, half:], part[:, :half]], axis=1)
             return part * cosine + swapped * sine
 
+        for load in small_loads:
+            load.wait()
         choice = routes_ref[...].astype(f32)
         down_at = lax.broadcasted_iota(jnp.int32, (64, 64), 0)
         across_at = lax.broadcasted_iota(jnp.int32, (64, 64), 1)
@@ -536,9 +552,16 @@
     return pl.pallas_call(
         kernel,
         out_shape=(jax.ShapeDtypeStruct((32, tokens.shape[1]), bf16), jax.ShapeDtypeStruct(tokens.shape, bf16)),
-        in_specs=[hbm] + [vmem] * 6 + [hbm] * 2 + [vmem] + [hbm] * 7,
+        in_specs=[hbm] * 17,
         out_specs=(vmem, vmem),
         scratch_shapes=[
+            pltpu.VMEM(moe_gain.shape, moe_gain.dtype),
+            pltpu.VMEM(routes.shape, routes.dtype),
+            pltpu.VMEM(group_prob.shape, group_prob.dtype),
+            pltpu.VMEM(expert_prob.shape, expert_prob.dtype),
+            pltpu.VMEM(within.shape, within.dtype),
+            pltpu.VMEM(starts.shape, starts.dtype),
+            pltpu.VMEM(latent_gain.shape, latent_gain.dtype),
             pltpu.VMEM(tokens.shape, bf16),
             pltpu.VMEM(latent.shape, bf16),
             pltpu.VMEM(rope_key.shape, bf16),
@@ -571,7 +594,7 @@
             pltpu.VMEM((2, 128, 256), f32),
             pltpu.VMEM((4, 32, 256), bf16),
             pltpu.VMEM((4, 32, 256), bf16),
-            pltpu.SemaphoreType.DMA((10,)),
+            pltpu.SemaphoreType.DMA((17,)),
             pltpu.SemaphoreType.DMA((1,)),
             pltpu.SemaphoreType.DMA((7, 4)),
             pltpu.SemaphoreType.DMA((ranks,)),

time: 113 us -> 112 us (level)
  no operation moved by 1% of the time
where the time goes in v6:
time: 112 us
  Pallas kernels  111 us (99%)
    pallas_call x1, Pallas kernels, exchange(): pl.pallas_call(kernel, out_shape=(jax.ShapeDtypeStruct((32, tokens.shape[...  110 us

profile of v6, /device:TPU:1, one launch (start us, length us, event | category | flops | bytes accessed | tf_op | source)
XLA Modules:
  0.0 112.1 jit_solution(14950297654131789112)
XLA Ops:
  0.6 109.6 %exchange.1 = (bf16[32,2048]{1,0:T(8,128)(2,1)}, bf16[64,2048]{1,0:T(8,128)(2,1)}) custom-call(bf16[64,2048]{1,0:T(8,128)(2,1)} %tok_hbm.1, f32[1,2048]{1,0:T(1,128)} %bitcast.11, s32[2,64]{1,0:T(2,128)} %bitcast.13, f32[1,64]{1,0:T(1,128)} %bitcast.15, f32[2,64]{1,0:T(2,128)} %bitcast.14, f32[128,64]{1,0:T(8,128)} %constant.4.clone.within_hbm, ...), custom_call_target="tpu_custom_call" | custom-call | flops 5000000000 | bytes 30000000 | tf_op jit(solution)/shard_map/exchange/pallas_call | solution.py:552
  110.3 1.8 %plain_copy.1 = (bf16[32,2048]{1,0:T(8,128)(2,1)}, bf16[64,2048]{1,0:T(8,128)(2,1)}) custom-call(bf16[32,2048]{1,0:T(8,128)(2,1)} %get-tuple-element.4.a_ref, bf16[64,2048]{1,0:T(8,128)(2,1)} %get-tuple-element.5.b_ref), custom_call_target="tpu_custom_call" | custom-call | tf_op jit(solution)/shard_map/plain_copy/pallas_call | solution.py:41

commit v7 on v6

--- a/solution.py
+++ b/solution.py
@@ -33,19 +33,39 @@
 
 
 def plain_copy(first, second):
-    def kernel(a_ref, b_ref, c_ref, d_ref):
-        c_ref[...] = a_ref[...]
-        d_ref[...] = b_ref[...]
-
-    vmem = pl.BlockSpec(memory_space=pltpu.VMEM)
+    half = second.shape[0] // 2
+
+    def kernel(a_ref, b_ref, c_ref, d_ref, held_a, held_b, load_sem, store_sem):
+        parts = (
+            (a_ref, held_a, c_ref),
+            (b_ref.at[:half], held_b.at[:half], d_ref.at[:half]),
+            (b_ref.at[half:], held_b.at[half:], d_ref.at[half:]),
+        )
+        loads = [pltpu.make_async_copy(p[0], p[1], load_sem.at[n]) for n, p in enumerate(parts)]
+        stores = [pltpu.make_async_copy(p[1], p[2], store_sem.at[n]) for n, p in enumerate(parts)]
+        for load in loads:
+            load.start()
+        for load, store in zip(loads, stores):
+            load.wait()
+            store.start()
+        for store in stores:
+            store.wait()
+
+    anywhere = pl.BlockSpec(memory_space=pl.ANY)
     return pl.pallas_call(
         kernel,
         out_shape=(
             jax.ShapeDtypeStruct(first.shape, first.dtype),
             jax.ShapeDtypeStruct(second.shape, second.dtype),
         ),
-        in_specs=[vmem, vmem],
-        out_specs=(vmem, vmem),
+        in_specs=[anywhere, anywhere],
+        out_specs=(anywhere, anywhere),
+        scratch_shapes=[
+            pltpu.VMEM(first.shape, first.dtype),
+            pltpu.VMEM(second.shape, second.dtype),
+            pltpu.SemaphoreType.DMA((3,)),
+            pltpu.SemaphoreType.DMA((3,)),
+        ],
         name="plain_copy",
     )(first, second)
 

time: 112 us -> 112 us (level)
  no operation moved by 1% of the time
where the time goes in v7:
time: 112 us
  Pallas kernels  111 us (99%)
    pallas_call x1, Pallas kernels, exchange(): pl.pallas_call(kernel, out_shape=(jax.ShapeDtypeStruct((32, tokens.shape[...  110 us

profile of v7, /device:TPU:1, one launch (start us, length us, event | category | flops | bytes accessed | tf_op | source)
XLA Modules:
  0.0 112.0 jit_solution(15405178896454303043)
XLA Ops:
  0.6 109.6 %exchange.1 = (bf16[32,2048]{1,0:T(8,128)(2,1)}, bf16[64,2048]{1,0:T(8,128)(2,1)}) custom-call(bf16[64,2048]{1,0:T(8,128)(2,1)} %tok_hbm.1, f32[1,2048]{1,0:T(1,128)} %bitcast.11, s32[2,64]{1,0:T(2,128)} %bitcast.13, f32[1,64]{1,0:T(1,128)} %bitcast.15, f32[2,64]{1,0:T(2,128)} %bitcast.14, f32[128,64]{1,0:T(8,128)} %constant.4.clone.within_hbm, ...), custom_call_target="tpu_custom_call" | custom-call | flops 5000000000 | bytes 30000000 | tf_op jit(solution)/shard_map/exchange/pallas_call | solution.py:572
  110.3 1.7 %plain_copy.1 = (bf16[32,2048]{1,0:T(8,128)(2,1)}, bf16[64,2048]{1,0:T(8,128)(2,1)}) custom-call(bf16[32,2048]{1,0:T(8,128)(2,1)} %get-tuple-element.4.a_ref, bf16[64,2048]{1,0:T(8,128)(2,1)} %get-tuple-element.5.b_ref), custom_call_target="tpu_custom_call" | custom-call | tf_op jit(solution)/shard_map/plain_copy/pallas_call | solution.py:55
